TPU v7x, 256 devices: a whole 4x4x8 slice. The times are simulated.
256 devices in a mesh: ep: 32 (over z, x), tp: 8 (over y, core).
Axes of the slice: x: 4, y: 4, z: 8, core: 2. Of those that a mesh axis runs over, the one named last changes fastest.
Arguments:
- out_gate: bfloat16 [32768, 2048], P(('ep', 'tp')), may hold values from -6 to 6
- in_gate: bfloat16 [32768, 2048], P(('ep', 'tp')), may hold values from -6 to 6
- values: bfloat16 [32768, 2048], P(('ep', 'tp')), may hold values from -6 to 6
- conv_taps: float32 [3, 2048], replicated, may hold values from -4 to 4
- out_weight: bfloat16 [2048, 2048], P(None, 'tp'), may hold values from -0.125 to 0.125
- expert_input: bfloat16 [65536, 2048], P(('ep', 'tp')), may hold values from -6 to 6
- norm_gain: float32 [2048], replicated, may hold values from 0.1 to 1.9
- expert_ids: int32 [65536, 2], P(('ep', 'tp')), may hold values from 0 to 31, all different within a row; in each aligned block of 256 rows (0 to 255, 256 to 511, ...) at most 32 rows name the same one
- route_logits: float32 [65536, 2], P(('ep', 'tp')), may hold values from -8 to 8
- group_share: float32 [65536], P(('ep', 'tp')), may hold values from 0.3 to 1
- gate_weight: bfloat16 [32, 2048, 512], P('ep'), may hold values from -0.125 to 0.125
- up_weight: bfloat16 [32, 2048, 512], P('ep'), may hold values from -0.125 to 0.125
- down_weight: bfloat16 [32, 512, 2048], P('ep'), may hold values from -0.25 to 0.25
Outputs:
- mixer_out: bfloat16 [32768, 2048], P(('ep', 'tp'))
- expert_mix: bfloat16 [65536, 2048], P(('ep', 'tp'))
Inputs may be any that keep to these rules, and one draw needn't show every extreme that they name: `expert_ids`: each row names 2 different experts. Within the rows of one device (aligned blocks of 256 rows) no expert is named by more than 32 rows, a bound that some block reaches.
All inputs are finite; a program needn't handle non-finite values.
Results may differ from a plain program's by a relative error of at most 0.0071.
Values may be sent and summed in bfloat16 or wider, within the bound.
A program may use at most 128 MiB of HBM per device.

v0:
```python
import jax
import jax.numpy as jnp
from jax import lax
from jax.sharding import PartitionSpec as P

SEQS = 1


norm_eps = 1e-05


def passed_along(value, axis, by):
    length = lax.axis_size(axis)
    pairs = [(i, i + by) for i in range(length) if 0 <= i + by < length]
    return lax.ppermute(value, axis, pairs)


def local(
    out_gate,
    in_gate,
    values,
    conv_taps,
    out_weight,
    expert_input,
    norm_gain,
    expert_ids,
    route_logits,
    group_share,
    gate_weight,
    up_weight,
    down_weight,
):
    rows_mix, width = out_gate.shape
    extent = conv_taps.shape[0] - 1
    gated = (in_gate.astype(jnp.float32) * values.astype(jnp.float32)).astype(jnp.bfloat16)
    before = passed_along(gated[rows_mix - extent :], ("ep", "tp"), 1)
    extended = jnp.concatenate([before, gated], axis=0)
    devices = lax.axis_size("ep") * lax.axis_size("tp")
    seq_len = devices * rows_mix // SEQS
    position = lax.axis_index(("ep", "tp")) * rows_mix + jnp.arange(rows_mix, dtype=jnp.int32)
    offset = position % seq_len
    filtered = jnp.zeros((rows_mix, width), jnp.float32)
    for delays in range(extent + 1):
        lagged = extended[extent - delays : extent - delays + rows_mix].astype(jnp.float32)
        if delays > 0:
            lagged = jnp.where((offset >= delays)[:, None], lagged, 0.0)
        filtered = filtered + conv_taps[extent - delays] * lagged
    mixed_rows = (out_gate.astype(jnp.float32) * filtered).astype(jnp.bfloat16)
    mixer_out = jnp.dot(
        mixed_rows,
        lax.all_gather(out_weight, "tp", axis=1, tiled=True),
        preferred_element_type=jnp.float32,
    ).astype(jnp.bfloat16)
    tokens, width = expert_input.shape
    chosen = expert_ids.shape[1]
    experts = lax.axis_size("ep") * gate_weight.shape[0]
    capacity = 2 * tokens * chosen // experts
    inputs = expert_input.astype(jnp.float32)
    scale = lax.rsqrt(jnp.mean(inputs * inputs, axis=-1, keepdims=True) + norm_eps)
    normed = (inputs * scale * norm_gain).astype(jnp.bfloat16)
    flat_ids = expert_ids.reshape(-1)
    entries = flat_ids.shape[0]
    one_hot = (flat_ids[:, None] == jnp.arange(experts, dtype=jnp.int32)[None, :]).astype(jnp.int32)
    earlier = jnp.cumsum(one_hot, axis=0) - one_hot
    slots = jnp.sum(earlier * one_hot, axis=1)
    target = flat_ids * capacity + slots
    owner = (
        jnp.zeros((experts * capacity,), jnp.int32)
        .at[target]
        .set(jnp.arange(entries, dtype=jnp.int32) // chosen)
    )
    filled = jnp.zeros((experts * capacity,), jnp.bfloat16).at[target].set(1.0)
    outgoing = (normed[owner] * filled[:, None]).reshape(experts, capacity, width)
    arrived = lax.all_to_all(outgoing, "ep", split_axis=0, concat_axis=0, tiled=True)
    rows = arrived.reshape(-1, width)
    gate = jnp.dot(rows, gate_weight[0], preferred_element_type=jnp.float32)
    upper = jnp.dot(rows, up_weight[0], preferred_element_type=jnp.float32)
    hidden = (jax.nn.silu(gate) * upper).astype(jnp.bfloat16)
    result = jnp.dot(hidden, down_weight[0], preferred_element_type=jnp.float32).astype(
        jnp.bfloat16
    )
    results = result.reshape(arrived.shape)
    returned = lax.all_to_all(results, "ep", split_axis=0, concat_axis=0, tiled=True)
    picked = returned.reshape(experts * capacity, width)[target].reshape(tokens, chosen, width)
    margin = route_logits[:, 0] - route_logits[:, 1]
    route_weight = group_share[:, None] * jnp.stack(
        [jax.nn.sigmoid(margin), jax.nn.sigmoid(-margin)], axis=1
    )
    expert_mix = jnp.sum(picked.astype(jnp.float32) * route_weight[:, :, None], axis=1).astype(
        jnp.bfloat16
    )
    return (mixer_out, expert_mix)


def solution(mesh):
    return jax.shard_map(
        local,
        mesh=mesh,
        in_specs=(
            P(("ep", "tp"), None),
            P(("ep", "tp"), None),
            P(("ep", "tp"), None),
            P(),
            P(None, "tp"),
            P(("ep", "tp"), None),
            P(),
            P(("ep", "tp"), None),
            P(("ep", "tp"), None),
            P(("ep", "tp")),
            P("ep", None, None),
            P("ep", None, None),
            P("ep", None, None),
        ),
        out_specs=(P(("ep", "tp"), None), P(("ep", "tp"), None)),
        check_vma=False,
    )
```

profile of v0, /device:TPU:160, one launch (start us, length us, event | category | flops | bytes accessed | tf_op | source)
XLA Modules:
  0.0 291.1 jit_solution(15468998242364581125)
XLA Ops:
  7.2 1.0 copy.17
  8.4 0.7 broadcast_multiply_fusion.1
  9.2 1.2 reduce-window.6
  10.3 0.2 slice_reduce_fusion
  10.7 0.1 mul.138
  11.0 2.4 scatter_custom_fusion
  13.5 1.5 fusion
  15.0 3.8 %scatter_custom_fusion.1 = bf16[1024]{0:T(1024)(128)(2,1)S(1)} fusion(s32[512]{0:T(512)S(1)} %bitcast.47, bf16[512]{0:T(512)(128)(2,1)S(1)} %broadcast.155, bf16[]{:T(256)} %constant.71.clone.1), kind=kCustom, calls=%fused_computation.61 | custom fusion | bytes 2050 | tf_op jit(solution)/shard_map/scatter | solution.py:72
  18.9 1.5 fusion.2
  20.4 6.0 %gather_fusion = bf16[1024,2048]{1,0:T(8,128)(2,1)} fusion(bf16[256,2048]{1,0:T(8,128)(2,1)S(1)} %fusion.2, s32[1024]{0:T(1024)S(1)} %fusion.24), kind=kCustom, calls=%fused_computation | custom fusion | bytes 8392704 | tf_op jit(solution)/shard_map/gather | solution.py:73
  26.4 4.5 %broadcast_multiply_fusion = bf16[32,32,2048]{2,1,0:T(8,128)(2,1)} fusion(bf16[32,32,2048]{2,1,0:T(8,128)(2,1)} %bitcast.44, bf16[32,32]{1,0:T(8,128)(2,1)S(1)} %mul.140), kind=kLoop, calls=%fused_computation.18 | loop fusion | flops 2097152 | bytes 8390656 | tf_op jit(solution)/shard_map/mul | solution.py:73
  30.9 9.4 %all-to-all-start = ((bf16[32,32,2048]{2,1,0:T(8,128)(2,1)}), bf16[32,32,2048]{2,1,0:T(8,128)(2,1)}, u32[]{:S(2)}, u32[]{:S(2)}) async-start(bf16[32,32,2048]{2,1,0:T(8,128)(2,1)} %broadcast_multiply_fusion), calls=%async_computation | async-start | bytes 8388608 | tf_op jit(solution)/shard_map/all_to_all | solution.py:74
  40.4 0.7 all-gather.2.cloned.1.call-update
  41.1 90.9 %all-to-all-done = bf16[32,32,2048]{2,1,0:T(8,128)(2,1)} async-done(((bf16[32,32,2048]{2,1,0:T(8,128)(2,1)}), bf16[32,32,2048]{2,1,0:T(8,128)(2,1)}, u32[]{:S(2)}, u32[]{:S(2)}) %all-to-all-start) | async-done | bytes 4194336 | tf_op jit(solution)/shard_map/all_to_all | solution.py:74
  132.0 6.6 %fusion.4 = f32[1024,512]{1,0:T(8,128)} fusion(bf16[1024,2048]{1,0:T(8,128)(2,1)} %bitcast.7, bf16[1,2048,512]{2,1,0:T(8,128)(2,1)} %param.24), kind=kOutput, calls=%fused_computation.13 | convolution fusion | flops 2147483648 | bytes 8388608 | tf_op jit(solution)/shard_map/dot_general | solution.py:77
  138.6 10.1 %convolution_convert_fusion = bf16[1024,2048]{1,0:T(8,128)(2,1)} fusion(bf16[1,512,2048]{2,1,0:T(8,128)(2,1)S(1)} %copy-done, f32[1024,512]{1,0:T(8,128)} %fusion.4, bf16[1024,2048]{1,0:T(8,128)(2,1)} %bitcast.7, bf16[1,2048,512]{2,1,0:T(8,128)(2,1)} %param.23), kind=kOutput, calls=%fused_computation.5 | convolution fusion | flops 4300210176 | bytes 14680064 | tf_op jit(solution)/shard_map/dot_general | solution.py:79
  148.6 9.8 %all-to-all-start.1 = ((bf16[32,32,2048]{2,1,0:T(8,128)(2,1)}), bf16[32,32,2048]{2,1,0:T(8,128)(2,1)}, u32[]{:S(2)}, u32[]{:S(2)}) async-start(bf16[32,32,2048]{2,1,0:T(8,128)(2,1)} %bitcast.45), calls=%async_computation.1 | async-start | bytes 8388608 | tf_op jit(solution)/shard_map/all_to_all | solution.py:83
  158.4 1.2 multiply_convert_fusion.2
  159.6 2.1 collective-permute-start
  162.0 92.9 %collective-permute-done = bf16[2,2048]{1,0:T(2,128)(2,1)S(1)} collective-permute-done((bf16[2,2048]{1,0:T(2,128)(2,1)S(1)}, bf16[2,2048]{1,0:T(2,128)(2,1)S(1)}, u32[]{:S(2)}, u32[]{:S(2)}) %collective-permute-start) | collective-permute-done | bytes 8224 | tf_op jit(solution)/shard_map/ppermute | solution.py:15
  255.0 6.0 %convolution_convert_fusion.1 = bf16[128,2048]{1,0:T(8,128)(2,1)} fusion(bf16[2048,2048]{1,0:T(8,128)(2,1)} %all-gather.2.cloned.1.call-done, bf16[128,2048]{1,0:T(8,128)(2,1)S(1)} %multiply_convert_fusion.2, bf16[128,2048]{1,0:T(8,128)(2,1)} %param.13, bf16[2,2048]{1,0:T(2,128)(2,1)S(1)} %collective-permute-done, f32[2048]{0:T(1024)S(1)} %bitcast.51, ...), kind=kOutput, calls=%fused_computation.8 | convolution fusion | flops 1078984704 | bytes 9994496 | tf_op jit(solution)/shard_map/dot_general | solution.py:49
  261.0 8.0 %gather_fusion.1 = bf16[512,2048]{1,0:T(8,128)(2,1)} fusion(bf16[1024,2048]{1,0:T(8,128)(2,1)} %bitcast.12, s32[1024]{0:T(1024)S(1)} %pad_clamp_fusion), kind=kCustom, calls=%fused_computation.1 | custom fusion | bytes 4196352 | tf_op jit(solution)/shard_map/gather | solution.py:84
  269.0 5.4 %reshape.132 = f32[256,2,2048]{2,1,0:T(2,128)} reshape(bf16[512,2048]{1,0:T(8,128)(2,1)} %gather_fusion.1) | data formatting | bytes 6291456 | tf_op jit(solution)/shard_map/convert_element_type | solution.py:89
  274.4 9.9 %multiply_reduce_fusion = bf16[256,2048]{1,0:T(8,128)(2,1)} fusion(f32[256,2,2048]{2,1,0:T(2,128)} %reshape.132, f32[256,2]{1,0:T(8,128)S(1)} %copy.20), kind=kLoop, calls=%fused_computation.4 | loop fusion | flops 1572864 | bytes 5244928 | tf_op jit(solution)/shard_map/reduce_sum | solution.py:89
  (36 shorter events, 1.0 us)
Async XLA Ops:
  7.2 131.4 %copy-start = (bf16[1,512,2048]{2,1,0:T(8,128)(2,1)S(1)}, bf16[1,512,2048]{2,1,0:T(8,128)(2,1)}, u32[]{:S(2)}) copy-start(bf16[1,512,2048]{2,1,0:T(8,128)(2,1)} %param.25) | copy-start | bytes 6291460
  7.2 11.7 %copy-start.3 = (f32[2048]{0:T(1024)S(1)}, f32[2048]{0:T(1024)}, u32[]{:S(2)}) copy-start(f32[2048]{0:T(1024)} %param.19) | copy-start | bytes 24580
  30.9 101.1 %all-to-all-start = ((bf16[32,32,2048]{2,1,0:T(8,128)(2,1)}), bf16[32,32,2048]{2,1,0:T(8,128)(2,1)}, u32[]{:S(2)}, u32[]{:S(2)}) async-start(bf16[32,32,2048]{2,1,0:T(8,128)(2,1)} %broadcast_multiply_fusion), calls=%async_computation | async-start | bytes 8388608 | tf_op jit(solution)/shard_map/all_to_all | solution.py:74
  40.3 214.6 %all-gather.2.cloned.1.call-start = ((), (), s32[]{:S(2)}) async-start(), calls=%async_computation.2 | async-start | bytes 9437184 | tf_op jit(solution)/shard_map/all_gather | solution.py:51
  148.6 9.8 %copy-start.1 = (bf16[128,2048]{1,0:T(8,128)(2,1)S(1)}, bf16[128,2048]{1,0:T(8,128)(2,1)}, u32[]{:S(2)}) copy-start(bf16[128,2048]{1,0:T(8,128)(2,1)} %param.15) | copy-start | bytes 1572868
  148.6 13.1 %copy-start.4 = (f32[256,2]{0,1:T(2,128)S(1)}, f32[256,2]{0,1:T(2,128)}, u32[]{:S(2)}) copy-start(f32[256,2]{0,1:T(2,128)} %param.21) | copy-start | bytes 6148
  148.6 13.2 %copy-start.5 = (f32[256]{0:T(256)S(1)}, f32[256]{0:T(256)}, u32[]{:S(2)}) copy-start(f32[256]{0:T(256)} %param.22) | copy-start | bytes 3076
  148.6 13.2 %copy-start.2 = (f32[3,2048]{1,0:T(4,128)S(1)}, f32[3,2048]{1,0:T(4,128)}, u32[]{:S(2)}) copy-start(f32[3,2048]{1,0:T(4,128)} %param.16) | copy-start | bytes 73732
  148.6 112.3 %all-to-all-start.1 = ((bf16[32,32,2048]{2,1,0:T(8,128)(2,1)}), bf16[32,32,2048]{2,1,0:T(8,128)(2,1)}, u32[]{:S(2)}, u32[]{:S(2)}) async-start(bf16[32,32,2048]{2,1,0:T(8,128)(2,1)} %bitcast.45), calls=%async_computation.1 | async-start | bytes 8388608 | tf_op jit(solution)/shard_map/all_to_all | solution.py:83
  159.6 95.3 %collective-permute-start = (bf16[2,2048]{1,0:T(2,128)(2,1)S(1)}, bf16[2,2048]{1,0:T(2,128)(2,1)S(1)}, u32[]{:S(2)}, u32[]{:S(2)}) collective-permute-start(bf16[2,2048]{1,0:T(2,128)(2,1)S(1)} %slice.44), channel_id=1, source_target_pairs={{0,1},{1,2},{2,3},{3,4},{4,5},{5,6},{6,7},{7,8},{8,9},{9,10},{10,1... | collective-permute-start | bytes 24584 | tf_op jit(solution)/shard_map/ppermute | solution.py:15
Sparse Core Ops, SparseCore 0:
  43.0 57.4 all-gather.1
where the time goes:
time: 292 us; the launch traced here: 291 us
  waiting for transfers between devices  185 us (63%)
  local copies, waits for them, and re-layouts  27.7 us (9%)
  matrix products  22.6 us (8%)
  starting transfers between devices  21.4 us (7%)
  other arithmetic  20.6 us (7%)
  between operations  14.3 us (5%)
    ppermute x1, waiting for transfers between devices, passed_along(): return lax.ppermute(value, axis, pairs)  92.9 us
    all_to_all x1, waiting for transfers between devices, local(): lax.all_to_all(outgoing, 'ep', split_axis=0, concat_axis=0, tiled=True)  90.9 us
    dot_general x1, matrix products, local(): jnp.dot(hidden, down_weight[0], preferred_element_type=jnp.float32)  10.1 us
    reduce_sum x1, other arithmetic, local(): jnp.sum(picked.astype(jnp.float32) * route_weight[:, :, None], axis=1)  9.86 us
    all_to_all x1, starting transfers between devices, local(): lax.all_to_all(results, 'ep', split_axis=0, concat_axis=0, tiled=True)  9.78 us
    all_to_all x1, starting transfers between devices, local(): lax.all_to_all(outgoing, 'ep', split_axis=0, concat_axis=0, tiled=True)  9.44 us
    gather x1, local copies, waits for them, and re-layouts, local(): returned.reshape(experts * capacity, width)[target]  8 us
    dot_general x1, matrix products, local(): upper = jnp.dot(rows, up_weight[0], preferred_element_type=jnp.float32)  6.56 us
  transfers between devices with their start and end apart: 4, of which 2 were waited for; matrix products, arithmetic and copies ran while one was open for 8% of the time, Pallas kernels for 0%

commit v1 on v0

v1 whole, which is shorter than its diff:
```python
import functools

import jax
import jax.numpy as jnp
from jax import lax
from jax.experimental import pallas as pl
from jax.experimental.pallas import tpu as pltpu
from jax.sharding import PartitionSpec as P

SEQS = 1
norm_eps = 1e-05
MESH = pl.DeviceIdType.MESH

NX, NY, NZ, NC = 4, 4, 8, 2
PLANE = NX * NY * NC
COLS = 512
GU_ROWS = 64
D_ROWS = 128


def moe_kernel(
    x_ref,
    gain_ref,
    ids_row_ref,
    ids_col_ref,
    logits_ref,
    share_ref,
    gate_hbm,
    up_hbm,
    down_hbm,
    out_ref,
    normed,
    combine,
    outgoing,
    rows,
    gu,
    down,
    acc,
    hidden,
    results,
    returned,
    w_sem,
    w_send,
    x_recv,
    x_send,
    r_recv,
    r_send,
):
    tokens, width = x_ref.shape
    cap = outgoing.shape[1] // PLANE
    chunks = width // COLS
    inner = hidden.shape[1]
    gu_hops = width // GU_ROWS
    d_hops = inner // D_ROWS

    ep, tp = lax.axis_index("ep"), lax.axis_index("tp")
    z, x = lax.div(ep, NX), lax.rem(ep, NX)
    y, c = lax.div(tp, NC), lax.rem(tp, NC)
    me = (c * NY + y) * NX + x
    ahead = lax.rem(z + 1, NZ) * NX + x
    behind = lax.rem(z + NZ - 1, NZ) * NX + x
    dist = lax.rem(z + NZ - (y + NY * c), NZ)
    is_home = dist == 0
    send_up = dist <= NZ // 2 - 1
    send_down = jnp.logical_or(dist == 0, dist >= NZ // 2 + 2)

    def peer(step):
        px = lax.rem(x + lax.rem(step, NX), NX)
        py = lax.rem(y + lax.rem(lax.div(step, NX), NY), NY)
        pc = lax.rem(c + lax.div(step, NX * NY), NC)
        return (pc * NY + py) * NX + px, z * NX + px, py * NC + pc

    def gu_at(i):
        return gu.at[pl.ds(pl.multiple_of(i * GU_ROWS, GU_ROWS), GU_ROWS), :]

    def down_at(j, i):
        return down.at[j, pl.ds(pl.multiple_of(i * D_ROWS, D_ROWS), D_ROWS), :]

    @pl.when(is_home)
    def _():
        def load_gu(i, _):
            at = pl.ds(pl.multiple_of(i * GU_ROWS, GU_ROWS), GU_ROWS)
            pltpu.make_async_copy(gate_hbm.at[0, at, :], gu.at[at, pl.ds(0, inner)], w_sem.at[i]).start()
            pltpu.make_async_copy(up_hbm.at[0, at, :], gu.at[at, pl.ds(inner, inner)], w_sem.at[i]).start()
            return 0

        lax.fori_loop(0, gu_hops, load_gu, 0)
        for j in range(chunks):
            for i in range(d_hops):
                pltpu.make_async_copy(
                    down_hbm.at[0, pl.ds(i * D_ROWS, D_ROWS), pl.ds(j * COLS, COLS)],
                    down.at[j, pl.ds(i * D_ROWS, D_ROWS), :],
                    w_sem.at[gu_hops + j * d_hops + i],
                ).start()

    barrier = pltpu.get_barrier_semaphore()

    def greet(step, _):
        _, pep, ptp = peer(step)
        pl.semaphore_signal(barrier, inc=1, device_id=(pep, ptp), device_id_type=MESH)
        return 0

    lax.fori_loop(1, PLANE, greet, 0)
    for other in (ahead, behind):
        pl.semaphore_signal(barrier, inc=1, device_id=(other, tp), device_id_type=MESH)

    xf = x_ref[...].astype(jnp.float32)
    scale = lax.rsqrt(jnp.mean(xf * xf, axis=-1, keepdims=True) + norm_eps)
    normed[...] = (xf * scale * gain_ref[...]).astype(jnp.bfloat16)

    expert_sub = lax.broadcasted_iota(jnp.int32, (PLANE, tokens), 0)
    t_sub = lax.broadcasted_iota(jnp.int32, (tokens, tokens), 0)
    t_lane = lax.broadcasted_iota(jnp.int32, (tokens, tokens), 1)
    earlier_cols = jnp.where(t_sub < t_lane, 1.0, 0.0).astype(jnp.bfloat16)
    earlier_rows = jnp.where(t_lane < t_sub, 1.0, 0.0).astype(jnp.bfloat16)

    id0, id1 = ids_row_ref[0:1, :], ids_row_ref[1:2, :]
    hot0 = jnp.where(expert_sub == id0, 1.0, 0.0)
    hot1 = jnp.where(expert_sub == id1, 1.0, 0.0)
    before0 = jnp.dot(hot0.astype(jnp.bfloat16), earlier_cols, preferred_element_type=jnp.float32)
    before1 = jnp.dot(hot1.astype(jnp.bfloat16), earlier_cols, preferred_element_type=jnp.float32)
    before1 = before1 + jnp.sum(hot0, axis=1, keepdims=True)
    place0 = id0 * cap + jnp.sum(hot0 * before0, axis=0, keepdims=True).astype(jnp.int32)
    place1 = id1 * cap + jnp.sum(hot1 * before1, axis=0, keepdims=True).astype(jnp.int32)

    def spread(block):
        row = block * 256 + lax.broadcasted_iota(jnp.int32, (256, tokens), 0)
        hit = jnp.logical_or(row == place0, row == place1)
        return jnp.where(hit, 1.0, 0.0).astype(jnp.bfloat16)

    def fill(k):
        for block in range(PLANE * cap // 256):
            outgoing[k, block * 256 : (block + 1) * 256, :] = jnp.dot(
                spread(block), normed[:, k * COLS : (k + 1) * COLS], preferred_element_type=jnp.float32
            ).astype(jnp.bfloat16)

    mine = pl.ds(pl.multiple_of(me * cap, cap), cap)

    def exchange(src, dst, k, send_sem, recv_sem):
        def one(step, _):
            j, pep, ptp = peer(step)
            pltpu.make_async_remote_copy(
                src_ref=src.at[k, pl.ds(pl.multiple_of(j * cap, cap), cap), :],
                dst_ref=dst.at[k, mine, :],
                send_sem=send_sem.at[k],
                recv_sem=recv_sem.at[k],
                device_id=(pep, ptp),
                device_id_type=MESH,
            ).start()
            return 0

        lax.fori_loop(1, PLANE, one, 0)
        dst[k, mine, :] = src[k, mine, :]

    def all_of(ref, k, sem):
        span = ref.at[k, pl.ds(0, (PLANE - 1) * cap), :]
        pltpu.make_async_copy(span, span, sem.at[k]).wait()

    def relay(part, sem, which):
        pltpu.make_async_copy(part, part, sem).wait()
        for go, other, way in ((send_up, ahead, 0), (send_down, behind, 1)):

            @pl.when(go)
            def _():
                pltpu.make_async_remote_copy(
                    src_ref=part,
                    dst_ref=part,
                    send_sem=w_send.at[way, which],
                    recv_sem=sem,
                    device_id=(other, tp),
                    device_id_type=MESH,
                ).start()

    def relay_gu(k):
        per = COLS // GU_ROWS

        def one(i, _):
            relay(gu_at(i), w_sem.at[i], 0)
            return 0

        lax.fori_loop(k * per, (k + 1) * per, one, 0)

    def relay_down(j):
        def one(i, _):
            relay(down_at(j, i), w_sem.at[gu_hops + j * d_hops + i], 1)
            return 0

        lax.fori_loop(0, d_hops, one, 0)

    def project(k):
        def one(n, _):
            at = pl.ds(pl.multiple_of(n * 256, 256), 256)
            part = jnp.dot(
                rows[k, :, :], gu[k * COLS : (k + 1) * COLS, at], preferred_element_type=jnp.float32
            )
            if k == 0:
                acc[:, at] = part
            else:
                acc[:, at] += part
            return 0

        lax.fori_loop(0, 2 * inner // 256, one, 0)

    def activate():
        def one(b, _):
            at = pl.ds(pl.multiple_of(b * 128, 128), 128)
            g, u = acc[at, 0:inner], acc[at, inner:]
            hidden[at, :] = (g * jax.nn.sigmoid(g) * u).astype(jnp.bfloat16)
            return 0

        lax.fori_loop(0, PLANE * cap // 128, one, 0)

    def produce(j):
        def one(n, _):
            at = pl.ds(pl.multiple_of(n * 256, 256), 256)
            results[j, :, at] = jnp.dot(
                hidden[...], down[j, :, at], preferred_element_type=jnp.float32
            ).astype(jnp.bfloat16)
            return 0

        lax.fori_loop(0, COLS // 256, one, 0)

    fill(0)
    pl.semaphore_wait(barrier, PLANE - 1 + 2)
    exchange(outgoing, rows, 0, x_send, x_recv)
    for k in range(1, chunks):
        fill(k)
        exchange(outgoing, rows, k, x_send, x_recv)

    expert_lane = lax.broadcasted_iota(jnp.int32, (tokens, 128), 1)
    cid0, cid1 = ids_col_ref[:, 0:1], ids_col_ref[:, 1:2]
    chot0 = jnp.where(expert_lane == cid0, 1.0, 0.0)
    chot1 = jnp.where(expert_lane == cid1, 1.0, 0.0)
    cbefore0 = jnp.dot(earlier_rows, chot0.astype(jnp.bfloat16), preferred_element_type=jnp.float32)
    cbefore1 = jnp.dot(earlier_rows, chot1.astype(jnp.bfloat16), preferred_element_type=jnp.float32)
    cbefore1 = cbefore1 + jnp.sum(chot0, axis=0, keepdims=True)
    cplace0 = cid0 * cap + jnp.sum(chot0 * cbefore0, axis=1, keepdims=True).astype(jnp.int32)
    cplace1 = cid1 * cap + jnp.sum(chot1 * cbefore1, axis=1, keepdims=True).astype(jnp.int32)
    margin = logits_ref[:, 0:1] - logits_ref[:, 1:2]
    weight0 = share_ref[...] * jax.nn.sigmoid(margin)
    weight1 = share_ref[...] * jax.nn.sigmoid(-margin)
    for block in range(PLANE * cap // 256):
        column = block * 256 + lax.broadcasted_iota(jnp.int32, (tokens, 256), 1)
        weight = jnp.where(column == cplace0, weight0, 0.0) + jnp.where(column == cplace1, weight1, 0.0)
        coarse = weight.astype(jnp.bfloat16)
        combine[0, :, block * 256 : (block + 1) * 256] = coarse
        combine[1, :, block * 256 : (block + 1) * 256] = (weight - coarse.astype(jnp.float32)).astype(jnp.bfloat16)

    relay_gu(0)
    for k in range(chunks):
        if k + 1 < chunks:
            relay_gu(k + 1)
        all_of(rows, k, x_recv)
        project(k)
    activate()
    for j in range(chunks):
        relay_down(j)
        produce(j)
        exchange(results, returned, j, r_send, r_recv)
    for j in range(chunks):
        all_of(returned, j, r_recv)
        mix = jnp.dot(combine[0], returned[j], preferred_element_type=jnp.float32)
        mix = mix + jnp.dot(combine[1], returned[j], preferred_element_type=jnp.float32)
        out_ref[:, j * COLS : (j + 1) * COLS] = mix.astype(jnp.bfloat16)

    for k in range(chunks):
        all_of(outgoing, k, x_send)
        all_of(results, k, r_send)
    for go, way in ((send_up, 0), (send_down, 1)):

        @pl.when(go)
        def _():
            pltpu.make_async_copy(gu, gu, w_send.at[way, 0]).wait()
            pltpu.make_async_copy(down, down, w_send.at[way, 1]).wait()


def moe(expert_input, norm_gain, expert_ids, route_logits, group_share, gate_weight, up_weight, down_weight):
    tokens, width = expert_input.shape
    inner = gate_weight.shape[2]
    cap = 2 * tokens * expert_ids.shape[1] // PLANE
    chunks = width // COLS
    slots = PLANE * cap
    hops = width // GU_ROWS + chunks * (inner // D_ROWS)
    vmem = pl.BlockSpec(memory_space=pltpu.VMEM)
    hbm = pl.BlockSpec(memory_space=pl.ANY)
    bf = jnp.bfloat16
    return pl.pallas_call(
        moe_kernel,
        out_shape=jax.ShapeDtypeStruct((tokens, width), bf),
        in_specs=[vmem] * 6 + [hbm] * 3,
        out_specs=vmem,
        scratch_shapes=[
            pltpu.VMEM((tokens, width), bf),
            pltpu.VMEM((2, tokens, slots), bf),
            pltpu.VMEM((chunks, slots, COLS), bf),
            pltpu.VMEM((chunks, slots, COLS), bf),
            pltpu.VMEM((width, 2 * inner), bf),
            pltpu.VMEM((chunks, inner, COLS), bf),
            pltpu.VMEM((slots, 2 * inner), jnp.float32),
            pltpu.VMEM((slots, inner), bf),
            pltpu.VMEM((chunks, slots, COLS), bf),
            pltpu.VMEM((chunks, slots, COLS), bf),
            pltpu.SemaphoreType.DMA((hops,)),
            pltpu.SemaphoreType.DMA((2, 2)),
            pltpu.SemaphoreType.DMA((chunks,)),
            pltpu.SemaphoreType.DMA((chunks,)),
            pltpu.SemaphoreType.DMA((chunks,)),
            pltpu.SemaphoreType.DMA((chunks,)),
        ],
        compiler_params=pltpu.CompilerParams(
            collective_id=0, has_side_effects=True, vmem_limit_bytes=60 * 1024 * 1024
        ),
        cost_estimate=pl.CostEstimate(flops=100_000_000_000, bytes_accessed=10_000_000, transcendentals=1_000_000),
        name="moe",
    )(
        expert_input,
        norm_gain[None, :],
        expert_ids.T,
        expert_ids,
        route_logits,
        group_share[:, None],
        gate_weight,
        up_weight,
        down_weight,
    )


def passed_along(value, axis, by):
    length = lax.axis_size(axis)
    pairs = [(i, i + by) for i in range(length) if 0 <= i + by < length]
    return lax.ppermute(value, axis, pairs)


def mixer(out_gate, in_gate, values, conv_taps, out_weight):
    rows_mix, width = out_gate.shape
    extent = conv_taps.shape[0] - 1
    gated = (in_gate.astype(jnp.float32) * values.astype(jnp.float32)).astype(jnp.bfloat16)
    before = passed_along(gated[rows_mix - extent :], ("ep", "tp"), 1)
    extended = jnp.concatenate([before, gated], axis=0)
    devices = lax.axis_size("ep") * lax.axis_size("tp")
    seq_len = devices * rows_mix // SEQS
    position = lax.axis_index(("ep", "tp")) * rows_mix + jnp.arange(rows_mix, dtype=jnp.int32)
    offset = position % seq_len
    filtered = jnp.zeros((rows_mix, width), jnp.float32)
    for delays in range(extent + 1):
        lagged = extended[extent - delays : extent - delays + rows_mix].astype(jnp.float32)
        if delays > 0:
            lagged = jnp.where((offset >= delays)[:, None], lagged, 0.0)
        filtered = filtered + conv_taps[extent - delays] * lagged
    mixed_rows = (out_gate.astype(jnp.float32) * filtered).astype(jnp.bfloat16)
    return jnp.dot(
        mixed_rows,
        lax.all_gather(out_weight, "tp", axis=1, tiled=True),
        preferred_element_type=jnp.float32,
    ).astype(jnp.bfloat16)


def local(
    out_gate,
    in_gate,
    values,
    conv_taps,
    out_weight,
    expert_input,
    norm_gain,
    expert_ids,
    route_logits,
    group_share,
    gate_weight,
    up_weight,
    down_weight,
):
    mixer_out = mixer(out_gate, in_gate, values, conv_taps, out_weight)
    expert_mix = moe(
        expert_input, norm_gain, expert_ids, route_logits, group_share, gate_weight, up_weight, down_weight
    )
    return (mixer_out, expert_mix)


def solution(mesh):
    return jax.shard_map(
        local,
        mesh=mesh,
        in_specs=(
            P(("ep", "tp"), None),
            P(("ep", "tp"), None),
            P(("ep", "tp"), None),
            P(),
            P(None, "tp"),
            P(("ep", "tp"), None),
            P(),
            P(("ep", "tp"), None),
            P(("ep", "tp"), None),
            P(("ep", "tp")),
            P("ep", None, None),
            P("ep", None, None),
            P("ep", None, None),
        ),
        out_specs=(P(("ep", "tp"), None), P(("ep", "tp"), None)),
        check_vma=False,
    )
```

time: 292 us -> 175 us (0.60)
  the two profiles are of different devices: /device:TPU:160 before, /device:TPU:8 now
where the time goes in v1:
time: 175 us; the launch traced here: 173 us
  Pallas kernels  136 us (78%)
  between operations  14.1 us (8%)
  waiting for transfers between devices  7.21 us (4%)
  local copies, waits for them, and re-layouts  6.3 us (4%)
  matrix products  5.89 us (3%)
  starting transfers between devices  1.96 us (1%)
    pallas_call x1, Pallas kernels, moe(): pl.pallas_call(moe_kernel, out_shape=jax.ShapeDtypeStruct((tokens, width)...  136 us
    all_gather x1, waiting for transfers between devices, mixer(): lax.all_gather(out_weight, 'tp', axis=1, tiled=True)  6.52 us
    dot_general x1, matrix products, mixer(): jnp.dot(mixed_rows, lax.all_gather(out_weight, 'tp', axis=1, tiled=True),...  5.89 us
    unnamed x7, local copies, waits for them, and re-layouts  3.93 us
  transfers between devices with their start and end apart: 2, of which 1 were waited for; matrix products, arithmetic and copies ran while one was open for 4% of the time, Pallas kernels for 79%

profile of v1, /device:TPU:8, one launch (start us, length us, event | category | flops | bytes accessed | tf_op | source)
XLA Modules:
  0.0 173.2 jit_solution(14253652024342491994)
XLA Ops:
  7.2 0.0 all-gather.2.cloned.1.call-start
  7.2 0.7 all-gather.2.cloned.1.call-update
  7.9 1.3 multiply_convert_fusion.1
  9.3 1.9 %collective-permute-start = (bf16[2,2048]{1,0:T(2,128)(2,1)S(1)}, bf16[2,2048]{1,0:T(2,128)(2,1)S(1)}, u32[]{:S(2)}, u32[]{:S(2)}) collective-permute-start(bf16[2,2048]{1,0:T(2,128)(2,1)S(1)} %slice.24), channel_id=1, source_target_pairs={{0,1},{1,2},{2,3},{3,4},{4,5},{5,6},{6,7},{7,8},{8,9},{9,10},{10,1... | collective-permute-start | bytes 24584 | tf_op jit(solution)/shard_map/ppermute | solution.py:331
  11.2 1.5 copy.17.ids_col_ref
  12.7 1.5 copy.18.logits_ref
  14.1 1.5 copy.19.share_ref
  15.6 0.9 fusion.11
  16.5 0.0 copy-start.1
  16.5 136.5 %moe.1 = bf16[256,2048]{1,0:T(8,128)(2,1)} custom-call(bf16[256,2048]{1,0:T(8,128)(2,1)} %x_ref.1, f32[1,2048]{1,0:T(1,128)} %bitcast.12, s32[2,256]{1,0:T(2,128)} %bitcast.10, s32[256,2]{1,0:T(8,128)} %copy.17.ids_col_ref, f32[256,2]{1,0:T(8,128)} %copy.18.logits_ref, f32[256,1]{1,0:T(8,128)} %copy.19.share_ref, bf16[1,2048,512]{2,1,0:T(8,128)(2,1)} %gate_hbm.1, ...), custom_call_target="tpu_custom_call" | custom-call | flops 99999997952 | bytes 10000000 | tf_op jit(solution)/shard_map/moe/pallas_call | solution.py:287
  153.0 0.0 collective-permute-done
  153.0 6.5 %all-gather.2.cloned.1.call-done = bf16[2048,2048]{1,0:T(8,128)(2,1)} async-done(((bf16[2048,256]{1,0:T(8,128)(2,1)}), bf16[2048,2048]{1,0:T(8,128)(2,1)}) %all-gather.2.cloned.1.call-update) | async-done | bytes 8388624 | tf_op jit(solution)/shard_map/all_gather | solution.py:353
  159.5 0.0 copy-done.1
  159.5 0.0 copy-start
  159.5 5.9 %convolution_convert_fusion = bf16[128,2048]{1,0:T(8,128)(2,1)} fusion(bf16[2048,2048]{1,0:T(8,128)(2,1)} %all-gather.2.cloned.1.call-done, bf16[128,2048]{1,0:T(8,128)(2,1)S(1)} %multiply_convert_fusion.1, bf16[128,2048]{1,0:T(8,128)(2,1)S(1)} %copy-done.1, bf16[2,2048]{1,0:T(2,128)(2,1)S(1)} %collective-permute-done, f32[2048]{0:T(1024)S(1)} %bitcast.8, ...), kind=kOutput, calls=%fused_computation | convolution fusion | flops 1078984704 | bytes 9994496 | tf_op jit(solution)/shard_map/dot_general | solution.py:351
  165.4 0.0 copy-done
  165.4 1.0 copy.21
  (2 shorter events, 0.0 us)
Async XLA Ops:
  7.2 152.4 %all-gather.2.cloned.1.call-start = ((), (), s32[]{:S(2)}) async-start(), calls=%async_computation | async-start | bytes 9437184 | tf_op jit(solution)/shard_map/all_gather | solution.py:353
  9.3 143.7 %collective-permute-start = (bf16[2,2048]{1,0:T(2,128)(2,1)S(1)}, bf16[2,2048]{1,0:T(2,128)(2,1)S(1)}, u32[]{:S(2)}, u32[]{:S(2)}) collective-permute-start(bf16[2,2048]{1,0:T(2,128)(2,1)S(1)} %slice.24), channel_id=1, source_target_pairs={{0,1},{1,2},{2,3},{3,4},{4,5},{5,6},{6,7},{7,8},{8,9},{9,10},{10,1... | collective-permute-start | bytes 24584 | tf_op jit(solution)/shard_map/ppermute | solution.py:331
  16.5 143.0 %copy-start.1 = (bf16[128,2048]{1,0:T(8,128)(2,1)S(1)}, bf16[128,2048]{1,0:T(8,128)(2,1)}, u32[]{:S(2)}) copy-start(bf16[128,2048]{1,0:T(8,128)(2,1)} %param.13) | copy-start | bytes 1572868
  159.5 5.9 %copy-start = (bf16[256,2048]{1,0:T(8,128)(2,1)S(1)}, bf16[256,2048]{1,0:T(8,128)(2,1)}, u32[]{:S(2)}) copy-start(bf16[256,2048]{1,0:T(8,128)(2,1)} %moe.1) | copy-start | bytes 3145732
Sparse Core Ops, SparseCore 0:
  9.8 149.6 all-gather.1

commit v2 on v1

v2 whole, which is shorter than its diff:
```python
import functools

import jax
import jax.numpy as jnp
from jax import lax
from jax.experimental import pallas as pl
from jax.experimental.pallas import tpu as pltpu
from jax.sharding import PartitionSpec as P

SEQS = 1
norm_eps = 1e-05
MESH = pl.DeviceIdType.MESH

NX, NY, NZ, NC = 4, 4, 8, 2
PLANE = NX * NY * NC
COLS = 512
GU_ROWS = 64
D_ROWS = 128


def step_kernel(
    x_ref,
    gain_ref,
    ids_ref,
    logits_ref,
    share_ref,
    taps_ref,
    og_hbm,
    ig_hbm,
    val_hbm,
    block_hbm,
    gate_hbm,
    up_hbm,
    down_hbm,
    mixer_ref,
    out_ref,
    normed,
    combine,
    outgoing,
    rows,
    gu,
    down,
    acc,
    hidden,
    results,
    returned,
    og,
    ig,
    val,
    gated,
    tail,
    halo,
    mixed,
    project_w,
    mixer_acc,
    w_sem,
    w_send,
    x_recv,
    x_send,
    r_recv,
    r_send,
    in_sem,
    halo_sem,
    share_sem,
    ring_recv,
    ring_send,
    pair_recv,
    pair_send,
):
    tokens, width = x_ref.shape
    cap = outgoing.shape[1] // PLANE
    chunks = width // COLS
    inner = hidden.shape[1]
    gu_hops = width // GU_ROWS
    d_hops = inner // D_ROWS
    rows_mix = og.shape[0]
    part = width // NZ

    ep, tp = lax.axis_index("ep"), lax.axis_index("tp")
    z, x = lax.div(ep, NX), lax.rem(ep, NX)
    y, c = lax.div(tp, NC), lax.rem(tp, NC)
    me = (c * NY + y) * NX + x
    ahead = lax.rem(z + 1, NZ) * NX + x
    behind = lax.rem(z + NZ - 1, NZ) * NX + x
    dist = lax.rem(z + NZ - (y + NY * c), NZ)
    is_home = dist == 0
    pair = y * NC + 1 - c
    n_ep, n_tp = NZ * NX, NY * NC
    flat = ep * n_tp + tp
    later = lax.rem(flat + 1, n_ep * n_tp)
    sooner = lax.rem(flat + n_ep * n_tp - 1, n_ep * n_tp)

    def peer(step):
        px = lax.rem(x + lax.rem(step, NX), NX)
        py = lax.rem(y + lax.rem(lax.div(step, NX), NY), NY)
        pc = lax.rem(c + lax.div(step, NX * NY), NC)
        return (pc * NY + py) * NX + px, z * NX + px, py * NC + pc

    def send(src, dst, send_sem, recv_sem, to):
        pltpu.make_async_remote_copy(
            src_ref=src,
            dst_ref=dst,
            send_sem=send_sem,
            recv_sem=recv_sem,
            device_id=to,
            device_id_type=MESH,
        ).start()

    def settle(ref, sem):
        pltpu.make_async_copy(ref, ref, sem).wait()

    def gu_at(i):
        return gu.at[pl.ds(pl.multiple_of(i * GU_ROWS, GU_ROWS), GU_ROWS), :]

    def down_at(j, i):
        return down.at[j, pl.ds(pl.multiple_of(i * D_ROWS, D_ROWS), D_ROWS), :]

    @pl.when(is_home)
    def _():
        def load_gu(i, _):
            at = pl.ds(pl.multiple_of(i * GU_ROWS, GU_ROWS), GU_ROWS)
            pltpu.make_async_copy(gate_hbm.at[0, at, :], gu.at[at, pl.ds(0, inner)], w_sem.at[i]).start()
            pltpu.make_async_copy(up_hbm.at[0, at, :], gu.at[at, pl.ds(inner, inner)], w_sem.at[i]).start()
            return 0

        lax.fori_loop(0, gu_hops, load_gu, 0)
        for j in range(chunks):
            for i in range(d_hops):
                pltpu.make_async_copy(
                    down_hbm.at[0, pl.ds(i * D_ROWS, D_ROWS), pl.ds(j * COLS, COLS)],
                    down.at[j, pl.ds(i * D_ROWS, D_ROWS), :],
                    w_sem.at[gu_hops + j * d_hops + i],
                ).start()

    loads = [
        pltpu.make_async_copy(ig_hbm, ig, in_sem.at[0]),
        pltpu.make_async_copy(val_hbm, val, in_sem.at[1]),
        pltpu.make_async_copy(og_hbm, og, in_sem.at[2]),
        pltpu.make_async_copy(block_hbm, project_w.at[tp], in_sem.at[3]),
    ]
    for load in loads:
        load.start()

    barrier = pltpu.get_barrier_semaphore()

    def greet(step, _):
        _, pep, ptp = peer(step)
        pl.semaphore_signal(barrier, inc=1, device_id=(pep, ptp), device_id_type=MESH)
        return 0

    lax.fori_loop(1, PLANE, greet, 0)
    for other in (ahead, behind):
        pl.semaphore_signal(barrier, inc=1, device_id=(other, tp), device_id_type=MESH)
    for other in (later, sooner):
        pl.semaphore_signal(
            barrier, inc=1, device_id=(lax.div(other, n_tp), lax.rem(other, n_tp)), device_id_type=MESH
        )

    xf = x_ref[...].astype(jnp.float32)
    scale = lax.rsqrt(jnp.mean(xf * xf, axis=-1, keepdims=True) + norm_eps)
    normed[...] = (xf * scale * gain_ref[...]).astype(jnp.bfloat16)

    loads[0].wait()
    loads[1].wait()
    product = (ig[...].astype(jnp.float32) * val[...].astype(jnp.float32)).astype(jnp.bfloat16)
    tail[...] = product[rows_mix - 16 :, :]
    gated[8:, :] = product.astype(jnp.float32)

    expert_sub = lax.broadcasted_iota(jnp.int32, (PLANE, tokens), 0)
    t_sub = lax.broadcasted_iota(jnp.int32, (tokens, tokens), 0)
    t_lane = lax.broadcasted_iota(jnp.int32, (tokens, tokens), 1)
    earlier = jnp.where(t_sub < t_lane, 1.0, 0.0).astype(jnp.bfloat16)
    id0, id1 = ids_ref[0:1, :], ids_ref[1:2, :]
    hot0 = jnp.where(expert_sub == id0, 1.0, 0.0)
    hot1 = jnp.where(expert_sub == id1, 1.0, 0.0)
    before0 = jnp.dot(hot0.astype(jnp.bfloat16), earlier, preferred_element_type=jnp.float32)
    before1 = jnp.dot(hot1.astype(jnp.bfloat16), earlier, preferred_element_type=jnp.float32)
    before1 = before1 + jnp.sum(hot0, axis=1, keepdims=True)
    slot0 = jnp.sum(hot0 * before0, axis=0, keepdims=True)
    slot1 = jnp.sum(hot1 * before1, axis=0, keepdims=True)
    place0 = id0 * cap + slot0.astype(jnp.int32)
    place1 = id1 * cap + slot1.astype(jnp.int32)

    def fill(k):
        for block in range(PLANE * cap // 256):
            row = block * 256 + lax.broadcasted_iota(jnp.int32, (256, tokens), 0)
            hit = jnp.logical_or(row == place0, row == place1)
            outgoing[k, block * 256 : (block + 1) * 256, :] = jnp.dot(
                jnp.where(hit, 1.0, 0.0).astype(jnp.bfloat16),
                normed[:, k * COLS : (k + 1) * COLS],
                preferred_element_type=jnp.float32,
            ).astype(jnp.bfloat16)

    mine = pl.ds(pl.multiple_of(me * cap, cap), cap)

    def exchange(src, dst, k, send_sem, recv_sem):
        dst[k, mine, :] = src[k, mine, :]

        def one(step, _):
            j, pep, ptp = peer(step)
            send(
                src.at[k, pl.ds(pl.multiple_of(j * cap, cap), cap), :],
                dst.at[k, mine, :],
                send_sem.at[k],
                recv_sem.at[k],
                (pep, ptp),
            )
            return 0

        lax.fori_loop(1, PLANE, one, 0)

    def all_of(ref, k, sem):
        settle(ref.at[k, pl.ds(0, (PLANE - 1) * cap), :], sem.at[k])

    half = NZ // 2

    def pass_on(piece, i, sem, which):
        up = jnp.logical_or(dist < half - 1, jnp.logical_and(dist == half - 1, lax.rem(i, 2) == 0))
        back = jnp.logical_or(
            jnp.logical_or(dist == 0, dist > half + 1), jnp.logical_and(dist == half + 1, lax.rem(i, 2) == 1)
        )
        for go, other, way in ((up, ahead, 0), (back, behind, 1)):

            @pl.when(go)
            def _():
                send(piece, piece, w_send.at[way, which], sem, (other, tp))

    def relay_gu(start, stop):
        def one(i, _):
            settle(gu_at(i), w_sem.at[i])
            pass_on(gu_at(i), i, w_sem.at[i], 0)
            return 0

        lax.fori_loop(start, stop, one, 0)

    def relay_down(j):
        def one(i, _):
            sem = w_sem.at[gu_hops + j * d_hops + i]
            settle(down_at(j, i), sem)
            pass_on(down_at(j, i), i, sem, 1)
            return 0

        lax.fori_loop(0, d_hops, one, 0)

    def project(k):
        def one(n, _):
            at = pl.ds(pl.multiple_of(n * 256, 256), 256)
            product = jnp.dot(rows[k, :, :], gu[k * COLS : (k + 1) * COLS, at], preferred_element_type=jnp.float32)
            if k == 0:
                acc[:, at] = product
            else:
                acc[:, at] += product
            return 0

        lax.fori_loop(0, 2 * inner // 256, one, 0)

    def activate():
        def one(b, _):
            at = pl.ds(pl.multiple_of(b * 128, 128), 128)
            g, u = acc[at, 0:inner], acc[at, inner:]
            hidden[at, :] = (g * jax.nn.sigmoid(g) * u).astype(jnp.bfloat16)
            return 0

        lax.fori_loop(0, PLANE * cap // 128, one, 0)

    def produce(j):
        def one(n, _):
            at = pl.ds(pl.multiple_of(n * 256, 256), 256)
            results[j, :, at] = jnp.dot(hidden[...], down[j, :, at], preferred_element_type=jnp.float32).astype(
                jnp.bfloat16
            )
            return 0

        lax.fori_loop(0, COLS // 256, one, 0)

    def mix(j):
        all_of(returned, j, r_recv)
        total = jnp.dot(combine[0], returned[j], preferred_element_type=jnp.float32)
        total = total + jnp.dot(combine[1], returned[j], preferred_element_type=jnp.float32)
        out_ref[:, j * COLS : (j + 1) * COLS] = total.astype(jnp.bfloat16)

    def near(i):
        return lax.rem(y + 1 + i, NY) * NC + c

    def share_of(b, q):
        return project_w.at[b, pl.ds(pl.multiple_of(q * part, part), part), :]

    others = NY - 1
    three = project_w.at[0, pl.ds(0, others * part), :]

    def to_pair(q):
        def one(i, _):
            send(share_of(near(i), q), share_of(near(i), q), pair_send.at[q], pair_recv.at[q], (ep, pair))
            return 0

        lax.fori_loop(0, others, one, 0)

    def goes_up(i):
        return jnp.logical_or(i == 0, jnp.logical_and(i == 2, c == 0))

    def ring_send_piece(q, way, m, i):
        other = ahead if way == 0 else behind
        piece = share_of(near(i), q)
        send(piece, piece, ring_send.at[way, m, i], ring_recv.at[way, m, i], (other, tp))

    def ring_start():
        def one(i, _):
            for way in (0, 1):
                ring_send_piece(z, way, 0, i)
            return 0

        lax.fori_loop(0, others, one, 0)

    def ring_step(k):
        for way in (0, 1):
            q = lax.rem(z + NZ - k, NZ) if way == 0 else lax.rem(z + k, NZ)

            def one(i, _):
                settle(share_of(near(i), q), ring_recv.at[way, k - 1, i])
                if k < half - 1:
                    ring_send_piece(q, way, k, i)
                else:

                    @pl.when(goes_up(i) if way == 0 else jnp.logical_not(goes_up(i)))
                    def _():
                        ring_send_piece(q, way, k, i)

                return 0

            lax.fori_loop(0, others, one, 0)
            to_pair(q)

    def ring_last():
        q = lax.rem(z + half, NZ)

        def one(i, _):
            @pl.when(goes_up(i))
            def _():
                settle(share_of(near(i), q), ring_recv.at[0, half - 1, i])

            @pl.when(jnp.logical_not(goes_up(i)))
            def _():
                settle(share_of(near(i), q), ring_recv.at[1, half - 1, i])

            return 0

        lax.fori_loop(0, others, one, 0)
        to_pair(q)

    def mixer_part(q, first=False):
        settle(three, pair_recv.at[q])
        at = pl.ds(pl.multiple_of(q * part, part), part)

        def one(b, _):
            to = pl.ds(pl.multiple_of(b * block_cols, block_cols), block_cols)
            product = jnp.dot(mixed[:, at], project_w[b, at, :], preferred_element_type=jnp.float32)
            if first:
                mixer_acc[:, to] = product
            else:
                mixer_acc[:, to] += product
            return 0

        lax.fori_loop(0, n_tp, one, 0)

    block_cols = project_w.shape[2]

    pl.semaphore_wait(barrier, PLANE - 1 + 4)
    send(tail, halo, halo_sem.at[0], halo_sem.at[1], (lax.div(later, n_tp), lax.rem(later, n_tp)))

    @pl.when(is_home)
    def _():
        relay_gu(0, 8)

    fill(0)
    exchange(outgoing, rows, 0, x_send, x_recv)
    fill(1)
    exchange(outgoing, rows, 1, x_send, x_recv)

    @pl.when(is_home)
    def _():
        relay_gu(8, gu_hops)
        for j in range(chunks):
            relay_down(j)

    away = jnp.logical_not(is_home)

    @pl.when(away)
    def _():
        relay_gu(0, 4)

    fill(2)
    exchange(outgoing, rows, 2, x_send, x_recv)

    @pl.when(away)
    def _():
        relay_gu(4, 8)

    fill(3)
    exchange(outgoing, rows, 3, x_send, x_recv)

    loads[3].wait()

    def give(i, _):
        piece = share_of(tp, z)
        send(piece, piece, share_sem.at[0], share_sem.at[1], (ep, near(i)))
        return 0

    lax.fori_loop(0, others, give, 0)
    send(project_w.at[tp], project_w.at[tp], pair_send.at[NZ], pair_recv.at[NZ], (ep, pair))

    @pl.when(away)
    def _():
        relay_gu(8, 12)

    margin = logits_ref[0:1, :] - logits_ref[1:2, :]
    weight0 = share_ref[...] * jax.nn.sigmoid(margin)
    weight1 = share_ref[...] * jax.nn.sigmoid(-margin)
    lane_rows = jnp.concatenate(
        [
            place0.astype(jnp.float32),
            place1.astype(jnp.float32),
            weight0,
            weight1,
            jnp.zeros((124, tokens), jnp.float32),
        ],
        axis=0,
    )
    turned = lane_rows.T
    cplace0, cplace1 = turned[:, 0:1].astype(jnp.int32), turned[:, 1:2].astype(jnp.int32)
    cweight0, cweight1 = turned[:, 2:3], turned[:, 3:4]
    for block in range(PLANE * cap // 256):
        column = block * 256 + lax.broadcasted_iota(jnp.int32, (tokens, 256), 1)
        weight = jnp.where(column == cplace0, cweight0, 0.0) + jnp.where(column == cplace1, cweight1, 0.0)
        coarse = weight.astype(jnp.bfloat16)
        combine[0, :, block * 256 : (block + 1) * 256] = coarse
        combine[1, :, block * 256 : (block + 1) * 256] = (weight - coarse.astype(jnp.float32)).astype(jnp.bfloat16)

    @pl.when(away)
    def _():
        relay_gu(12, 16)

    all_of(rows, 0, x_recv)
    project(0)

    settle(halo, halo_sem.at[1])
    loads[2].wait()
    seq_len = n_ep * n_tp * rows_mix // SEQS
    inside = lax.rem(flat * rows_mix, seq_len) != 0
    early = halo[...].astype(jnp.float32)[8:, :]
    gated[0:8, :] = jnp.where(inside, early, 0.0)

    def filter_columns(n, _):
        at = pl.ds(pl.multiple_of(n * 256, 256), 256)
        filtered = taps_ref[0:1, at] * gated[6 : 6 + rows_mix, at]
        filtered = filtered + taps_ref[1:2, at] * gated[7 : 7 + rows_mix, at]
        filtered = filtered + taps_ref[2:3, at] * gated[8 : 8 + rows_mix, at]
        mixed[:, at] = (og[:, at].astype(jnp.float32) * filtered).astype(jnp.bfloat16)
        return 0

    lax.fori_loop(0, width // 256, filter_columns, 0)

    @pl.when(away)
    def _():
        relay_gu(16, 24)

    all_of(rows, 1, x_recv)
    project(1)

    @pl.when(away)
    def _():
        relay_gu(24, 32)

    all_of(rows, 2, x_recv)
    project(2)
    all_of(rows, 3, x_recv)
    project(3)
    activate()
    for j in range(chunks):

        @pl.when(away)
        def _():
            relay_down(j)

        produce(j)
        exchange(results, returned, j, r_send, r_recv)

    settle(three, share_sem.at[1])
    ring_start()
    to_pair(z)
    settle(project_w.at[tp], pair_recv.at[NZ])
    mixer_part(z, first=True)
    ring_step(1)
    ring_step(2)
    mix(0)
    mixer_part(lax.rem(z + NZ - 1, NZ))
    mixer_part(lax.rem(z + 1, NZ))
    ring_step(3)
    mix(1)
    mixer_part(lax.rem(z + NZ - 2, NZ))
    mixer_part(lax.rem(z + 2, NZ))
    ring_last()
    mixer_part(lax.rem(z + NZ - 3, NZ))
    mixer_part(lax.rem(z + 3, NZ))
    mix(2)
    mixer_part(lax.rem(z + half, NZ))
    mixer_ref[...] = mixer_acc[...].astype(jnp.bfloat16)
    mix(3)

    for k in range(chunks):
        all_of(outgoing, k, x_send)
        all_of(results, k, r_send)
    settle(tail, halo_sem.at[0])
    settle(three, share_sem.at[0])
    settle(project_w.at[tp], pair_send.at[NZ])

    def pairs_left(q, _):
        settle(three, pair_send.at[q])
        return 0

    lax.fori_loop(0, NZ, pairs_left, 0)

    def rings_left(i, _):
        for way in (0, 1):
            for m in range(half - 1):
                settle(share_of(0, 0), ring_send.at[way, m, i])

        @pl.when(goes_up(i))
        def _():
            settle(share_of(0, 0), ring_send.at[0, half - 1, i])

        @pl.when(jnp.logical_not(goes_up(i)))
        def _():
            settle(share_of(0, 0), ring_send.at[1, half - 1, i])

        return 0

    lax.fori_loop(0, others, rings_left, 0)

    def weights_left(way, which, some):
        ref = gu if which == 0 else down
        if some:
            ref = gu.at[pl.ds(0, width // 2), :] if which == 0 else down.at[pl.ds(0, chunks // 2), :, :]
        settle(ref, w_send.at[way, which])

    for way, full, some in (
        (0, dist < half - 1, dist == half - 1),
        (1, jnp.logical_or(dist == 0, dist > half + 1), dist == half + 1),
    ):

        @pl.when(full)
        def _():
            weights_left(way, 0, False)
            weights_left(way, 1, False)

        @pl.when(some)
        def _():
            weights_left(way, 0, True)
            weights_left(way, 1, True)


def local(
    out_gate,
    in_gate,
    values,
    conv_taps,
    out_weight,
    expert_input,
    norm_gain,
    expert_ids,
    route_logits,
    group_share,
    gate_weight,
    up_weight,
    down_weight,
):
    tokens, width = expert_input.shape
    inner = gate_weight.shape[2]
    rows_mix = out_gate.shape[0]
    cap = 2 * tokens * expert_ids.shape[1] // PLANE
    chunks = width // COLS
    slots = PLANE * cap
    hops = width // GU_ROWS + chunks * (inner // D_ROWS)
    vmem = pl.BlockSpec(memory_space=pltpu.VMEM)
    hbm = pl.BlockSpec(memory_space=pl.ANY)
    bf, dma = jnp.bfloat16, pltpu.SemaphoreType.DMA
    return pl.pallas_call(
        step_kernel,
        out_shape=(
            jax.ShapeDtypeStruct((rows_mix, width), bf),
            jax.ShapeDtypeStruct((tokens, width), bf),
        ),
        in_specs=[vmem] * 6 + [hbm] * 7,
        out_specs=(vmem, vmem),
        scratch_shapes=[
            pltpu.VMEM((tokens, width), bf),
            pltpu.VMEM((2, tokens, slots), bf),
            pltpu.VMEM((chunks, slots, COLS), bf),
            pltpu.VMEM((chunks, slots, COLS), bf),
            pltpu.VMEM((width, 2 * inner), bf),
            pltpu.VMEM((chunks, inner, COLS), bf),
            pltpu.VMEM((slots, 2 * inner), jnp.float32),
            pltpu.VMEM((slots, inner), bf),
            pltpu.VMEM((chunks, slots, COLS), bf),
            pltpu.VMEM((chunks, slots, COLS), bf),
            pltpu.VMEM((rows_mix, width), bf),
            pltpu.VMEM((rows_mix, width), bf),
            pltpu.VMEM((rows_mix, width), bf),
            pltpu.VMEM((8 + rows_mix, width), jnp.float32),
            pltpu.VMEM((16, width), bf),
            pltpu.VMEM((16, width), bf),
            pltpu.VMEM((rows_mix, width), bf),
            pltpu.VMEM((NY * NC, *out_weight.shape), bf),
            pltpu.VMEM((rows_mix, width), jnp.float32),
            dma((hops,)),
            dma((2, 2)),
            dma((chunks,)),
            dma((chunks,)),
            dma((chunks,)),
            dma((chunks,)),
            dma((4,)),
            dma((2,)),
            dma((2,)),
            dma((2, NZ // 2, NY - 1)),
            dma((2, NZ // 2, NY - 1)),
            dma((NZ + 1,)),
            dma((NZ + 1,)),
        ],
        compiler_params=pltpu.CompilerParams(
            collective_id=0, has_side_effects=True, vmem_limit_bytes=63 * 1024 * 1024
        ),
        name="layer_step",
    )(
        expert_input,
        norm_gain[None, :],
        expert_ids.T,
        route_logits.T,
        group_share[None, :],
        conv_taps,
        out_gate,
        in_gate,
        values,
        out_weight,
        gate_weight,
        up_weight,
        down_weight,
    )


def solution(mesh):
    return jax.shard_map(
        local,
        mesh=mesh,
        in_specs=(
            P(("ep", "tp"), None),
            P(("ep", "tp"), None),
            P(("ep", "tp"), None),
            P(),
            P(None, "tp"),
            P(("ep", "tp"), None),
            P(),
            P(("ep", "tp"), None),
            P(("ep", "tp"), None),
            P(("ep", "tp")),
            P("ep", None, None),
            P("ep", None, None),
            P("ep", None, None),
        ),
        out_specs=(P(("ep", "tp"), None), P(("ep", "tp"), None)),
        check_vma=False,
    )
```

time: 175 us -> 144 us (0.82)
  the two profiles are of different devices: /device:TPU:8 before, /device:TPU:96 now
where the time goes in v2:
time: 144 us; the launch traced here: 143 us
  Pallas kernels  138 us (96%)
  local copies, waits for them, and re-layouts  4.18 us (3%)
    pallas_call x1, Pallas kernels, local(): pl.pallas_call(step_kernel, out_shape=(jax.ShapeDtypeStruct((rows_mix, wi...  138 us
    unnamed x2, local copies, waits for them, and re-layouts  4.18 us

profile of v2, /device:TPU:96, one launch (start us, length us, event | category | flops | bytes accessed | tf_op | source)
XLA Modules:
  0.0 143.3 jit_solution(1037305789431914548)
XLA Ops:
  0.6 138.5 %layer_step.1 = (bf16[128,2048]{1,0:T(8,128)(2,1)}, bf16[256,2048]{1,0:T(8,128)(2,1)}) custom-call(bf16[256,2048]{1,0:T(8,128)(2,1)} %x_ref.1, f32[1,2048]{1,0:T(1,128)} %bitcast.4, s32[2,256]{1,0:T(2,128)} %bitcast.5, f32[2,256]{1,0:T(2,128)} %bitcast.6, f32[1,256]{1,0:T(1,128)} %bitcast.7, f32[3,2048]{1,0:T(4,128)} %taps_ref.1, bf16[128,2048]{1,0:T(8,128)(2,1)} %og_hbm.1, ...), custom_call_target="tpu_custom_call" | custom-call | tf_op jit(solution)/shard_map/layer_step/pallas_call | solution.py:586
  139.1 1.9 %copy.17 = bf16[128,2048]{1,0:T(8,128)(2,1)} copy(bf16[128,2048]{1,0:T(8,128)(2,1)} %get-tuple-element.4) | data formatting | bytes 1048576
  141.0 2.3 %copy.18 = bf16[256,2048]{1,0:T(8,128)(2,1)} copy(bf16[256,2048]{1,0:T(8,128)(2,1)} %get-tuple-element.5) | data formatting | bytes 2097152

commit v3 on v2

--- a/solution.py
+++ b/solution.py
@@ -14,8 +14,9 @@
 NX, NY, NZ, NC = 4, 4, 8, 2
 PLANE = NX * NY * NC
 COLS = 512
-GU_ROWS = 64
-D_ROWS = 128
+GU_ROWS = 32
+D_ROWS = 64
+WINDOW = 6
 
 
 def step_kernel(
@@ -32,6 +33,8 @@
     gate_hbm,
     up_hbm,
     down_hbm,
+    mixer_hbm,
+    out_hbm,
     mixer_ref,
     out_ref,
     normed,
@@ -66,6 +69,9 @@
     ring_send,
     pair_recv,
     pair_send,
+    along_recv,
+    along_send,
+    out_sem,
 ):
     tokens, width = x_ref.shape
     cap = outgoing.shape[1] // PLANE
@@ -74,7 +80,8 @@
     gu_hops = width // GU_ROWS
     d_hops = inner // D_ROWS
     rows_mix = og.shape[0]
-    part = width // NZ
+    split, plain = width // 2, width // 4
+    part, wide = split // NZ, (width - split - plain) // NX
 
     ep, tp = lax.axis_index("ep"), lax.axis_index("tp")
     z, x = lax.div(ep, NX), lax.rem(ep, NX)
@@ -115,6 +122,21 @@
     def down_at(j, i):
         return down.at[j, pl.ds(pl.multiple_of(i * D_ROWS, D_ROWS), D_ROWS), :]
 
+    barrier = pltpu.get_barrier_semaphore()
+
+    def greet(step, _):
+        _, pep, ptp = peer(step)
+        pl.semaphore_signal(barrier, inc=1, device_id=(pep, ptp), device_id_type=MESH)
+        return 0
+
+    lax.fori_loop(1, PLANE, greet, 0)
+    for other in (ahead, behind):
+        pl.semaphore_signal(barrier, inc=1, device_id=(other, tp), device_id_type=MESH)
+    for other in (later, sooner):
+        pl.semaphore_signal(
+            barrier, inc=1, device_id=(lax.div(other, n_tp), lax.rem(other, n_tp)), device_id_type=MESH
+        )
+
     @pl.when(is_home)
     def _():
         def load_gu(i, _):
@@ -140,21 +162,6 @@
     ]
     for load in loads:
         load.start()
-
-    barrier = pltpu.get_barrier_semaphore()
-
-    def greet(step, _):
-        _, pep, ptp = peer(step)
-        pl.semaphore_signal(barrier, inc=1, device_id=(pep, ptp), device_id_type=MESH)
-        return 0
-
-    lax.fori_loop(1, PLANE, greet, 0)
-    for other in (ahead, behind):
-        pl.semaphore_signal(barrier, inc=1, device_id=(other, tp), device_id_type=MESH)
-    for other in (later, sooner):
-        pl.semaphore_signal(
-            barrier, inc=1, device_id=(lax.div(other, n_tp), lax.rem(other, n_tp)), device_id_type=MESH
-        )
 
     xf = x_ref[...].astype(jnp.float32)
     scale = lax.rsqrt(jnp.mean(xf * xf, axis=-1, keepdims=True) + norm_eps)
@@ -214,35 +221,47 @@
 
     half = NZ // 2
 
-    def pass_on(piece, i, sem, which):
-        up = jnp.logical_or(dist < half - 1, jnp.logical_and(dist == half - 1, lax.rem(i, 2) == 0))
-        back = jnp.logical_or(
-            jnp.logical_or(dist == 0, dist > half + 1), jnp.logical_and(dist == half + 1, lax.rem(i, 2) == 1)
-        )
-        for go, other, way in ((up, ahead, 0), (back, behind, 1)):
-
-            @pl.when(go)
+    def pass_on(piece, t, sem):
+        def one(number, other, way):
+            slot = lax.rem(number, WINDOW)
+
+            @pl.when(number >= WINDOW)
             def _():
-                send(piece, piece, w_send.at[way, which], sem, (other, tp))
-
-    def relay_gu(start, stop):
-        def one(i, _):
-            settle(gu_at(i), w_sem.at[i])
-            pass_on(gu_at(i), i, w_sem.at[i], 0)
-            return 0
-
-        lax.fori_loop(start, stop, one, 0)
-
-    def relay_down(j):
-        def one(i, _):
-            sem = w_sem.at[gu_hops + j * d_hops + i]
-            settle(down_at(j, i), sem)
-            pass_on(down_at(j, i), i, sem, 1)
-            return 0
-
-        lax.fori_loop(0, d_hops, one, 0)
-
-    def project(k):
+                settle(piece, w_send.at[way, slot])
+
+            send(piece, piece, w_send.at[way, slot], sem, (other, tp))
+
+        for all_way, some_way, other, way in (
+            (dist < half - 1, dist == half - 1, ahead, 0),
+            (jnp.logical_or(dist == 0, dist > half + 1), dist == half + 1, behind, 1),
+        ):
+
+            @pl.when(all_way)
+            def _():
+                one(t, other, way)
+
+            @pl.when(jnp.logical_and(some_way, lax.rem(t, 2) == way))
+            def _():
+                one(lax.div(t, 2), other, way)
+
+    def serve(start, stop):
+        def gate_up(t, _):
+            settle(gu_at(t), w_sem.at[t])
+            pass_on(gu_at(t), t, w_sem.at[t])
+            return 0
+
+        def downward(t, _):
+            j, i = lax.div(t - gu_hops, d_hops), lax.rem(t - gu_hops, d_hops)
+            settle(down_at(j, i), w_sem.at[t])
+            pass_on(down_at(j, i), t, w_sem.at[t])
+            return 0
+
+        if start < gu_hops:
+            lax.fori_loop(start, min(stop, gu_hops), gate_up, 0)
+        if stop > gu_hops:
+            lax.fori_loop(max(start, gu_hops), stop, downward, 0)
+
+    def project(k, piece):
         def one(n, _):
             at = pl.ds(pl.multiple_of(n * 256, 256), 256)
             product = jnp.dot(rows[k, :, :], gu[k * COLS : (k + 1) * COLS, at], preferred_element_type=jnp.float32)
@@ -252,7 +271,8 @@
                 acc[:, at] += product
             return 0
 
-        lax.fori_loop(0, 2 * inner // 256, one, 0)
+        steps = 2 * inner // 256 // 2
+        lax.fori_loop(piece * steps, (piece + 1) * steps, one, 0)
 
     def activate():
         def one(b, _):
@@ -278,6 +298,8 @@
         total = jnp.dot(combine[0], returned[j], preferred_element_type=jnp.float32)
         total = total + jnp.dot(combine[1], returned[j], preferred_element_type=jnp.float32)
         out_ref[:, j * COLS : (j + 1) * COLS] = total.astype(jnp.bfloat16)
+        columns = pl.ds(j * COLS, COLS)
+        pltpu.make_async_copy(out_ref.at[:, columns], out_hbm.at[:, columns], out_sem.at[j]).start()
 
     def near(i):
         return lax.rem(y + 1 + i, NY) * NC + c
@@ -287,10 +309,53 @@
 
     others = NY - 1
     three = project_w.at[0, pl.ds(0, others * part), :]
+    three_wide = project_w.at[0, pl.ds(0, others * wide), :]
+
+    def wide_of(b, q):
+        return project_w.at[b, pl.ds(pl.multiple_of(split + q * wide, wide), wide), :]
+
+    lone, whole = NZ + NX, NZ + NX + 1
+    three_plain = project_w.at[0, pl.ds(0, others * plain), :]
+
+    def plain_of(b):
+        return project_w.at[b, pl.ds(width - plain, plain), :]
 
     def to_pair(q):
         def one(i, _):
             send(share_of(near(i), q), share_of(near(i), q), pair_send.at[q], pair_recv.at[q], (ep, pair))
+            return 0
+
+        lax.fori_loop(0, others, one, 0)
+
+    def wide_to_pair(q):
+        def one(i, _):
+            send(wide_of(near(i), q), wide_of(near(i), q), pair_send.at[NZ + q], pair_recv.at[NZ + q], (ep, pair))
+            return 0
+
+        lax.fori_loop(0, others, one, 0)
+
+    def along_x():
+        settle(three_wide, share_sem.at[3])
+
+        def one(t, _):
+            far, i = lax.div(t, others), lax.rem(t, others)
+            to = z * NX + lax.rem(x + 1 + far, NX)
+            send(wide_of(near(i), x), wide_of(near(i), x), along_send.at[far], along_recv.at[far], (to, tp))
+            return 0
+
+        lax.fori_loop(0, (NX - 1) * others, one, 0)
+        wide_to_pair(x)
+
+    def from_x():
+        for far in range(NX - 1):
+            settle(three_wide, along_recv.at[far])
+            wide_to_pair(lax.rem(x + NX - 1 - far, NX))
+
+    def from_y():
+        settle(three_plain, share_sem.at[5])
+
+        def one(i, _):
+            send(plain_of(near(i)), plain_of(near(i)), pair_send.at[lone], pair_recv.at[lone], (ep, pair))
             return 0
 
         lax.fori_loop(0, others, one, 0)
@@ -347,70 +412,36 @@
         lax.fori_loop(0, others, one, 0)
         to_pair(q)
 
-    def mixer_part(q, first=False):
+    def mixer_wide():
+        for q in range(NX):
+            settle(three_wide, pair_recv.at[NZ + q])
+        settle(three_plain, pair_recv.at[lone])
+
+        def one(b, _):
+            to = pl.ds(pl.multiple_of(b * block_cols, block_cols), block_cols)
+            mixer_acc[:, to] = jnp.dot(
+                mixed[:, split:], project_w[b, split:, :], preferred_element_type=jnp.float32
+            )
+            return 0
+
+        lax.fori_loop(0, n_tp, one, 0)
+
+    def mixer_part(q):
         settle(three, pair_recv.at[q])
         at = pl.ds(pl.multiple_of(q * part, part), part)
 
         def one(b, _):
             to = pl.ds(pl.multiple_of(b * block_cols, block_cols), block_cols)
-            product = jnp.dot(mixed[:, at], project_w[b, at, :], preferred_element_type=jnp.float32)
-            if first:
-                mixer_acc[:, to] = product
-            else:
-                mixer_acc[:, to] += product
+            mixer_acc[:, to] += jnp.dot(mixed[:, at], project_w[b, at, :], preferred_element_type=jnp.float32)
             return 0
 
         lax.fori_loop(0, n_tp, one, 0)
 
     block_cols = project_w.shape[2]
 
-    pl.semaphore_wait(barrier, PLANE - 1 + 4)
-    send(tail, halo, halo_sem.at[0], halo_sem.at[1], (lax.div(later, n_tp), lax.rem(later, n_tp)))
-
-    @pl.when(is_home)
-    def _():
-        relay_gu(0, 8)
-
-    fill(0)
-    exchange(outgoing, rows, 0, x_send, x_recv)
-    fill(1)
-    exchange(outgoing, rows, 1, x_send, x_recv)
-
-    @pl.when(is_home)
-    def _():
-        relay_gu(8, gu_hops)
-        for j in range(chunks):
-            relay_down(j)
-
-    away = jnp.logical_not(is_home)
-
-    @pl.when(away)
-    def _():
-        relay_gu(0, 4)
-
-    fill(2)
-    exchange(outgoing, rows, 2, x_send, x_recv)
-
-    @pl.when(away)
-    def _():
-        relay_gu(4, 8)
-
-    fill(3)
-    exchange(outgoing, rows, 3, x_send, x_recv)
-
-    loads[3].wait()
-
-    def give(i, _):
-        piece = share_of(tp, z)
-        send(piece, piece, share_sem.at[0], share_sem.at[1], (ep, near(i)))
-        return 0
-
-    lax.fori_loop(0, others, give, 0)
-    send(project_w.at[tp], project_w.at[tp], pair_send.at[NZ], pair_recv.at[NZ], (ep, pair))
-
-    @pl.when(away)
-    def _():
-        relay_gu(8, 12)
+    first = WINDOW
+    for k in range(chunks):
+        fill(k)
 
     margin = logits_ref[0:1, :] - logits_ref[1:2, :]
     weight0 = share_ref[...] * jax.nn.sigmoid(margin)
@@ -435,12 +466,45 @@
         combine[0, :, block * 256 : (block + 1) * 256] = coarse
         combine[1, :, block * 256 : (block + 1) * 256] = (weight - coarse.astype(jnp.float32)).astype(jnp.bfloat16)
 
-    @pl.when(away)
+    pl.semaphore_wait(barrier, PLANE - 1 + 4)
+    send(tail, halo, halo_sem.at[0], halo_sem.at[1], (lax.div(later, n_tp), lax.rem(later, n_tp)))
+
+    @pl.when(is_home)
     def _():
-        relay_gu(12, 16)
-
+        serve(0, first)
+
+    for k in range(chunks):
+        exchange(outgoing, rows, k, x_send, x_recv)
+
+    loads[3].wait()
+
+    def give(i, _):
+        for piece, k in ((share_of(tp, z), 0), (wide_of(tp, x), 2)):
+            send(piece, piece, share_sem.at[k], share_sem.at[k + 1], (ep, near(i)))
+        return 0
+
+    lax.fori_loop(0, others, give, 0)
+
+    def give_plain(i, _):
+        send(plain_of(tp), plain_of(tp), share_sem.at[4], share_sem.at[5], (ep, near(i)))
+        return 0
+
+    lax.fori_loop(0, others, give_plain, 0)
+    send(project_w.at[tp], project_w.at[tp], pair_send.at[whole], pair_recv.at[whole], (ep, pair))
+
+    @pl.when(jnp.logical_not(is_home))
+    def _():
+        serve(0, first)
+
+    def upto(fraction):
+        return gu_hops * fraction // 32
+
+    serve(first, upto(10))
     all_of(rows, 0, x_recv)
-    project(0)
+    project(0, 0)
+    serve(upto(10), upto(11))
+    project(0, 1)
+    serve(upto(11), upto(13))
 
     settle(halo, halo_sem.at[1])
     loads[2].wait()
@@ -459,39 +523,42 @@
 
     lax.fori_loop(0, width // 256, filter_columns, 0)
 
-    @pl.when(away)
-    def _():
-        relay_gu(16, 24)
-
+    serve(upto(13), upto(19))
     all_of(rows, 1, x_recv)
-    project(1)
-
-    @pl.when(away)
-    def _():
-        relay_gu(24, 32)
-
+    project(1, 0)
+    serve(upto(19), upto(20))
+    project(1, 1)
+    serve(upto(20), upto(27))
     all_of(rows, 2, x_recv)
-    project(2)
+    project(2, 0)
+    serve(upto(27), upto(28))
+    project(2, 1)
+    serve(upto(28), gu_hops + d_hops // 2)
     all_of(rows, 3, x_recv)
-    project(3)
+    along_x()
+    project(3, 0)
+    serve(gu_hops + d_hops // 2, gu_hops + d_hops * 3 // 4)
+    project(3, 1)
+    serve(gu_hops + d_hops * 3 // 4, gu_hops + d_hops)
     activate()
     for j in range(chunks):
-
-        @pl.when(away)
-        def _():
-            relay_down(j)
-
+        if j > 0:
+            serve(gu_hops + j * d_hops, gu_hops + (j + 1) * d_hops)
+        if j == chunks - 1:
+            settle(three, share_sem.at[1])
+            ring_start()
         produce(j)
         exchange(results, returned, j, r_send, r_recv)
 
-    settle(three, share_sem.at[1])
-    ring_start()
     to_pair(z)
-    settle(project_w.at[tp], pair_recv.at[NZ])
-    mixer_part(z, first=True)
+    from_y()
+    from_x()
+    settle(project_w.at[tp], pair_recv.at[whole])
     ring_step(1)
+    mix(0)
+    mixer_wide()
+    mixer_part(z)
     ring_step(2)
-    mix(0)
     mixer_part(lax.rem(z + NZ - 1, NZ))
     mixer_part(lax.rem(z + 1, NZ))
     ring_step(3)
@@ -504,6 +571,8 @@
     mix(2)
     mixer_part(lax.rem(z + half, NZ))
     mixer_ref[...] = mixer_acc[...].astype(jnp.bfloat16)
+    mixer_out = pltpu.make_async_copy(mixer_ref, mixer_hbm, out_sem.at[chunks])
+    mixer_out.start()
     mix(3)
 
     for k in range(chunks):
@@ -511,7 +580,14 @@
         all_of(results, k, r_send)
     settle(tail, halo_sem.at[0])
     settle(three, share_sem.at[0])
-    settle(project_w.at[tp], pair_send.at[NZ])
+    settle(three_wide, share_sem.at[2])
+    settle(three_plain, share_sem.at[4])
+    settle(three_plain, pair_send.at[lone])
+    settle(project_w.at[tp], pair_send.at[whole])
+    for q in range(NX):
+        settle(three_wide, pair_send.at[NZ + q])
+    for far in range(NX - 1):
+        settle(three_wide, along_send.at[far])
 
     def pairs_left(q, _):
         settle(three, pair_send.at[q])
@@ -536,26 +612,20 @@
 
     lax.fori_loop(0, others, rings_left, 0)
 
-    def weights_left(way, which, some):
-        ref = gu if which == 0 else down
-        if some:
-            ref = gu.at[pl.ds(0, width // 2), :] if which == 0 else down.at[pl.ds(0, chunks // 2), :, :]
-        settle(ref, w_send.at[way, which])
-
-    for way, full, some in (
-        (0, dist < half - 1, dist == half - 1),
-        (1, jnp.logical_or(dist == 0, dist > half + 1), dist == half + 1),
+    for sends, way in (
+        (dist < half, 0),
+        (jnp.logical_or(dist == 0, dist > half), 1),
     ):
 
-        @pl.when(full)
+        @pl.when(sends)
         def _():
-            weights_left(way, 0, False)
-            weights_left(way, 1, False)
-
-        @pl.when(some)
-        def _():
-            weights_left(way, 0, True)
-            weights_left(way, 1, True)
+            for slot in range(WINDOW):
+                settle(gu_at(0), w_send.at[way, slot])
+
+    mixer_out.wait()
+    for j in range(chunks):
+        columns = pl.ds(j * COLS, COLS)
+        pltpu.make_async_copy(out_ref.at[:, columns], out_hbm.at[:, columns], out_sem.at[j]).wait()
 
 
 def local(
@@ -590,8 +660,10 @@
             jax.ShapeDtypeStruct((tokens, width), bf),
         ),
         in_specs=[vmem] * 6 + [hbm] * 7,
-        out_specs=(vmem, vmem),
+        out_specs=(hbm, hbm),
         scratch_shapes=[
+            pltpu.VMEM((rows_mix, width), bf),
+            pltpu.VMEM((tokens, width), bf),
             pltpu.VMEM((tokens, width), bf),
             pltpu.VMEM((2, tokens, slots), bf),
             pltpu.VMEM((chunks, slots, COLS), bf),
@@ -612,18 +684,21 @@
             pltpu.VMEM((NY * NC, *out_weight.shape), bf),
             pltpu.VMEM((rows_mix, width), jnp.float32),
             dma((hops,)),
-            dma((2, 2)),
+            dma((2, WINDOW)),
             dma((chunks,)),
             dma((chunks,)),
             dma((chunks,)),
             dma((chunks,)),
             dma((4,)),
             dma((2,)),
-            dma((2,)),
+            dma((6,)),
             dma((2, NZ // 2, NY - 1)),
             dma((2, NZ // 2, NY - 1)),
-            dma((NZ + 1,)),
-            dma((NZ + 1,)),
+            dma((NZ + NX + 2,)),
+            dma((NZ + NX + 2,)),
+            dma((NX - 1,)),
+            dma((NX - 1,)),
+            dma((chunks + 1,)),
         ],
         compiler_params=pltpu.CompilerParams(
             collective_id=0, has_side_effects=True, vmem_limit_bytes=63 * 1024 * 1024

time: 144 us -> 136 us (0.944)
  the two profiles are of different devices: /device:TPU:96 before, /device:TPU:8 now
where the time goes in v3:
time: 136 us; the launch traced here: 135 us
  Pallas kernels  131 us (96%)
  local copies, waits for them, and re-layouts  4.18 us (3%)
    pallas_call x1, Pallas kernels, local(): pl.pallas_call(step_kernel, out_shape=(jax.ShapeDtypeStruct((rows_mix, wi...  131 us
    unnamed x2, local copies, waits for them, and re-layouts  4.18 us

profile of v3, /device:TPU:8, one launch (start us, length us, event | category | flops | bytes accessed | tf_op | source)
XLA Modules:
  0.0 135.4 jit_solution(10438432751892616385)
XLA Ops:
  0.6 130.5 %layer_step.1 = (bf16[128,2048]{1,0:T(8,128)(2,1)}, bf16[256,2048]{1,0:T(8,128)(2,1)}) custom-call(bf16[256,2048]{1,0:T(8,128)(2,1)} %x_ref.1, f32[1,2048]{1,0:T(1,128)} %bitcast.4, s32[2,256]{1,0:T(2,128)} %bitcast.5, f32[2,256]{1,0:T(2,128)} %bitcast.6, f32[1,256]{1,0:T(1,128)} %bitcast.7, f32[3,2048]{1,0:T(4,128)} %taps_ref.1, bf16[128,2048]{1,0:T(8,128)(2,1)} %og_hbm.1, ...), custom_call_target="tpu_custom_call" | custom-call | tf_op jit(solution)/shard_map/layer_step/pallas_call | solution.py:656
  131.2 1.9 %copy.17 = bf16[128,2048]{1,0:T(8,128)(2,1)} copy(bf16[128,2048]{1,0:T(8,128)(2,1)} %get-tuple-element.4) | data formatting | bytes 1048576
  133.1 2.3 %copy.18 = bf16[256,2048]{1,0:T(8,128)(2,1)} copy(bf16[256,2048]{1,0:T(8,128)(2,1)} %get-tuple-element.5) | data formatting | bytes 2097152

commit v4 on v3

--- a/solution.py
+++ b/solution.py
@@ -33,8 +33,6 @@
     gate_hbm,
     up_hbm,
     down_hbm,
-    mixer_hbm,
-    out_hbm,
     mixer_ref,
     out_ref,
     normed,
@@ -71,7 +69,6 @@
     pair_send,
     along_recv,
     along_send,
-    out_sem,
 ):
     tokens, width = x_ref.shape
     cap = outgoing.shape[1] // PLANE
@@ -298,8 +295,6 @@
         total = jnp.dot(combine[0], returned[j], preferred_element_type=jnp.float32)
         total = total + jnp.dot(combine[1], returned[j], preferred_element_type=jnp.float32)
         out_ref[:, j * COLS : (j + 1) * COLS] = total.astype(jnp.bfloat16)
-        columns = pl.ds(j * COLS, COLS)
-        pltpu.make_async_copy(out_ref.at[:, columns], out_hbm.at[:, columns], out_sem.at[j]).start()
 
     def near(i):
         return lax.rem(y + 1 + i, NY) * NC + c
@@ -412,30 +407,29 @@
         lax.fori_loop(0, others, one, 0)
         to_pair(q)
 
-    def mixer_wide():
+    def mixer_part(begin, end, last):
+        def one(b, _):
+            to = pl.ds(pl.multiple_of(b * block_cols, block_cols), block_cols)
+            product = jnp.dot(mixed[:, begin:end], project_w[b, begin:end, :], preferred_element_type=jnp.float32)
+            if last:
+                mixer_ref[:, to] = (mixer_acc[:, to] + product).astype(jnp.bfloat16)
+            else:
+                mixer_acc[:, to] = product
+            return 0
+
+        lax.fori_loop(0, n_tp, one, 0)
+
+    def mixer_second():
         for q in range(NX):
             settle(three_wide, pair_recv.at[NZ + q])
         settle(three_plain, pair_recv.at[lone])
-
-        def one(b, _):
-            to = pl.ds(pl.multiple_of(b * block_cols, block_cols), block_cols)
-            mixer_acc[:, to] = jnp.dot(
-                mixed[:, split:], project_w[b, split:, :], preferred_element_type=jnp.float32
-            )
-            return 0
-
-        lax.fori_loop(0, n_tp, one, 0)
-
-    def mixer_part(q):
-        settle(three, pair_recv.at[q])
-        at = pl.ds(pl.multiple_of(q * part, part), part)
-
-        def one(b, _):
-            to = pl.ds(pl.multiple_of(b * block_cols, block_cols), block_cols)
-            mixer_acc[:, to] += jnp.dot(mixed[:, at], project_w[b, at, :], preferred_element_type=jnp.float32)
-            return 0
-
-        lax.fori_loop(0, n_tp, one, 0)
+        settle(project_w.at[tp], pair_recv.at[whole])
+        mixer_part(split, width, False)
+
+    def mixer_first():
+        for q in range(NZ):
+            settle(three, pair_recv.at[q])
+        mixer_part(0, split, True)
 
     block_cols = project_w.shape[2]
 
@@ -473,14 +467,18 @@
     def _():
         serve(0, first)
 
+    def give_wide(i, _):
+        send(wide_of(tp, x), wide_of(tp, x), share_sem.at[2], share_sem.at[3], (ep, near(i)))
+        return 0
+
     for k in range(chunks):
         exchange(outgoing, rows, k, x_send, x_recv)
-
-    loads[3].wait()
+        if k == 0:
+            loads[3].wait()
+            lax.fori_loop(0, others, give_wide, 0)
 
     def give(i, _):
-        for piece, k in ((share_of(tp, z), 0), (wide_of(tp, x), 2)):
-            send(piece, piece, share_sem.at[k], share_sem.at[k + 1], (ep, near(i)))
+        send(share_of(tp, z), share_of(tp, z), share_sem.at[0], share_sem.at[1], (ep, near(i)))
         return 0
 
     lax.fori_loop(0, others, give, 0)
@@ -499,12 +497,7 @@
     def upto(fraction):
         return gu_hops * fraction // 32
 
-    serve(first, upto(10))
-    all_of(rows, 0, x_recv)
-    project(0, 0)
-    serve(upto(10), upto(11))
-    project(0, 1)
-    serve(upto(11), upto(13))
+    serve(first, upto(14))
 
     settle(halo, halo_sem.at[1])
     loads[2].wait()
@@ -523,19 +516,24 @@
 
     lax.fori_loop(0, width // 256, filter_columns, 0)
 
-    serve(upto(13), upto(19))
+    serve(upto(14), upto(18))
+    all_of(rows, 0, x_recv)
+    project(0, 0)
+    serve(upto(18), upto(19))
+    project(0, 1)
+    serve(upto(19), upto(26))
+    along_x()
+    serve(upto(26), upto(30))
     all_of(rows, 1, x_recv)
     project(1, 0)
-    serve(upto(19), upto(20))
+    serve(upto(30), upto(31))
     project(1, 1)
-    serve(upto(20), upto(27))
+    serve(upto(31), gu_hops + d_hops // 4)
     all_of(rows, 2, x_recv)
     project(2, 0)
-    serve(upto(27), upto(28))
+    serve(gu_hops + d_hops // 4, gu_hops + d_hops // 2)
     project(2, 1)
-    serve(upto(28), gu_hops + d_hops // 2)
     all_of(rows, 3, x_recv)
-    along_x()
     project(3, 0)
     serve(gu_hops + d_hops // 2, gu_hops + d_hops * 3 // 4)
     project(3, 1)
@@ -551,28 +549,17 @@
         exchange(results, returned, j, r_send, r_recv)
 
     to_pair(z)
+    ring_step(1)
+    from_x()
+    ring_step(2)
+    ring_step(3)
     from_y()
-    from_x()
-    settle(project_w.at[tp], pair_recv.at[whole])
-    ring_step(1)
     mix(0)
-    mixer_wide()
-    mixer_part(z)
-    ring_step(2)
-    mixer_part(lax.rem(z + NZ - 1, NZ))
-    mixer_part(lax.rem(z + 1, NZ))
-    ring_step(3)
+    ring_last()
+    mixer_second()
     mix(1)
-    mixer_part(lax.rem(z + NZ - 2, NZ))
-    mixer_part(lax.rem(z + 2, NZ))
-    ring_last()
-    mixer_part(lax.rem(z + NZ - 3, NZ))
-    mixer_part(lax.rem(z + 3, NZ))
+    mixer_first()
     mix(2)
-    mixer_part(lax.rem(z + half, NZ))
-    mixer_ref[...] = mixer_acc[...].astype(jnp.bfloat16)
-    mixer_out = pltpu.make_async_copy(mixer_ref, mixer_hbm, out_sem.at[chunks])
-    mixer_out.start()
     mix(3)
 
     for k in range(chunks):
@@ -621,11 +608,6 @@
         def _():
             for slot in range(WINDOW):
                 settle(gu_at(0), w_send.at[way, slot])
-
-    mixer_out.wait()
-    for j in range(chunks):
-        columns = pl.ds(j * COLS, COLS)
-        pltpu.make_async_copy(out_ref.at[:, columns], out_hbm.at[:, columns], out_sem.at[j]).wait()
 
 
 def local(
@@ -651,7 +633,7 @@
     slots = PLANE * cap
     hops = width // GU_ROWS + chunks * (inner // D_ROWS)
     vmem = pl.BlockSpec(memory_space=pltpu.VMEM)
-    hbm = pl.BlockSpec(memory_space=pl.ANY)
+    hbm = pl.BlockSpec(memory_space=pltpu.HBM)
     bf, dma = jnp.bfloat16, pltpu.SemaphoreType.DMA
     return pl.pallas_call(
         step_kernel,
@@ -660,10 +642,8 @@
             jax.ShapeDtypeStruct((tokens, width), bf),
         ),
         in_specs=[vmem] * 6 + [hbm] * 7,
-        out_specs=(hbm, hbm),
+        out_specs=(vmem, vmem),
         scratch_shapes=[
-            pltpu.VMEM((rows_mix, width), bf),
-            pltpu.VMEM((tokens, width), bf),
             pltpu.VMEM((tokens, width), bf),
             pltpu.VMEM((2, tokens, slots), bf),
             pltpu.VMEM((chunks, slots, COLS), bf),
@@ -698,13 +678,12 @@
             dma((NZ + NX + 2,)),
             dma((NX - 1,)),
             dma((NX - 1,)),
-            dma((chunks + 1,)),
         ],
         compiler_params=pltpu.CompilerParams(
-            collective_id=0, has_side_effects=True, vmem_limit_bytes=63 * 1024 * 1024
+            collective_id=0, has_side_effects=True, vmem_limit_bytes=48 * 1024 * 1024
         ),
         name="layer_step",
-    )(
+    )(*(pltpu.with_memory_space_constraint(value, pltpu.HBM) for value in (
         expert_input,
         norm_gain[None, :],
         expert_ids.T,
@@ -718,7 +697,7 @@
         gate_weight,
         up_weight,
         down_weight,
-    )
+    )))
 
 
 def solution(mesh):

time: 136 us -> 127 us (0.934)
  Pallas kernels: 131 us -> 124 us
  local copies, waits for them, and re-layouts: 4.18 us -> 1.77 us
    pallas_call x1, Pallas kernels: 131 us -> 124 us  [local(): pl.pallas_call(step_kernel, out_shape=(jax.ShapeDtypeStruct((rows_mix, wi...]
    unnamed x2, local copies, waits for them, and re-layouts: 4.18 us -> 1.77 us
where the time goes in v4:
time: 127 us; the launch traced here: 126 us
  Pallas kernels  124 us (98%)
  local copies, waits for them, and re-layouts  1.77 us (1%)
    pallas_call x1, Pallas kernels, local(): pl.pallas_call(step_kernel, out_shape=(jax.ShapeDtypeStruct((rows_mix, wi...  124 us

profile of v4, /device:TPU:8, one launch (start us, length us, event | category | flops | bytes accessed | tf_op | source)
XLA Modules:
  0.0 126.2 jit_solution(5100455073297449391)
XLA Ops:
  0.6 123.8 %layer_step.1 = (bf16[128,2048]{1,0:T(8,128)(2,1)S(1)}, bf16[256,2048]{1,0:T(8,128)(2,1)S(1)}) custom-call(bf16[256,2048]{1,0:T(8,128)(2,1)} %x_ref.1, f32[1,2048]{1,0:T(1,128)} %bitcast.4, s32[2,256]{1,0:T(2,128)} %bitcast.5, f32[2,256]{1,0:T(2,128)} %bitcast.6, f32[1,256]{1,0:T(1,128)} %bitcast.7, f32[3,2048]{1,0:T(4,128)} %taps_ref.1, ...), custom_call_target="tpu_custom_call" | custom-call | tf_op jit(solution)/shard_map/layer_step/pallas_call | solution.py:638
  124.5 0.8 copy.17
  125.3 1.0 copy.18

commit v5 on v4

--- a/solution.py
+++ b/solution.py
@@ -560,8 +560,6 @@
     mix(1)
     mixer_first()
     mix(2)
-    mix(3)
-
     for k in range(chunks):
         all_of(outgoing, k, x_send)
         all_of(results, k, r_send)
@@ -608,6 +606,8 @@
         def _():
             for slot in range(WINDOW):
                 settle(gu_at(0), w_send.at[way, slot])
+
+    mix(3)
 
 
 def local(

time: 127 us -> 127 us (level)
  no operation moved by 1% of the time
where the time goes in v5:
time: 127 us; the launch traced here: 126 us
  Pallas kernels  124 us (98%)
  local copies, waits for them, and re-layouts  1.77 us (1%)
    pallas_call x1, Pallas kernels, local(): pl.pallas_call(step_kernel, out_shape=(jax.ShapeDtypeStruct((rows_mix, wi...  124 us

profile of v5, /device:TPU:8, one launch (start us, length us, event | category | flops | bytes accessed | tf_op | source)
XLA Modules:
  0.0 126.2 jit_solution(6859539554661426517)
XLA Ops:
  0.6 123.8 %layer_step.1 = (bf16[128,2048]{1,0:T(8,128)(2,1)S(1)}, bf16[256,2048]{1,0:T(8,128)(2,1)S(1)}) custom-call(bf16[256,2048]{1,0:T(8,128)(2,1)} %x_ref.1, f32[1,2048]{1,0:T(1,128)} %bitcast.4, s32[2,256]{1,0:T(2,128)} %bitcast.5, f32[2,256]{1,0:T(2,128)} %bitcast.6, f32[1,256]{1,0:T(1,128)} %bitcast.7, f32[3,2048]{1,0:T(4,128)} %taps_ref.1, ...), custom_call_target="tpu_custom_call" | custom-call | tf_op jit(solution)/shard_map/layer_step/pallas_call | solution.py:638
  124.5 0.8 copy.17
  125.3 1.0 copy.18

commit v6 on v5

--- a/solution.py
+++ b/solution.py
@@ -555,8 +555,8 @@
     ring_step(3)
     from_y()
     mix(0)
+    mixer_second()
     ring_last()
-    mixer_second()
     mix(1)
     mixer_first()
     mix(2)

time: 127 us -> 127 us (level)
  no operation moved by 1% of the time
where the time goes in v6:
time: 127 us
  Pallas kernels  125 us (98%)
  local copies, waits for them, and re-layouts  1.77 us (1%)
    pallas_call x1, Pallas kernels, local(): pl.pallas_call(step_kernel, out_shape=(jax.ShapeDtypeStruct((rows_mix, wi...  125 us

profile of v6, /device:TPU:8, one launch (start us, length us, event | category | flops | bytes accessed | tf_op | source)
XLA Modules:
  0.0 127.2 jit_solution(1117504533136654497)
XLA Ops:
  0.6 124.8 %layer_step.1 = (bf16[128,2048]{1,0:T(8,128)(2,1)S(1)}, bf16[256,2048]{1,0:T(8,128)(2,1)S(1)}) custom-call(bf16[256,2048]{1,0:T(8,128)(2,1)} %x_ref.1, f32[1,2048]{1,0:T(1,128)} %bitcast.4, s32[2,256]{1,0:T(2,128)} %bitcast.5, f32[2,256]{1,0:T(2,128)} %bitcast.6, f32[1,256]{1,0:T(1,128)} %bitcast.7, f32[3,2048]{1,0:T(4,128)} %taps_ref.1, ...), custom_call_target="tpu_custom_call" | custom-call | tf_op jit(solution)/shard_map/layer_step/pallas_call | solution.py:638
  125.4 0.8 copy.17
  126.2 1.0 copy.18
